TPU v7x, 32 devices: a whole 2x2x4 slice. The times are simulated.
32 devices in a mesh: fs: 8 (over z, y), tp: 4 (over x, core).
Axes of the slice: x: 2, y: 2, z: 4, core: 2. Of those that a mesh axis runs over, the one named last changes fastest.
Arguments:
- tokens: bfloat16 [640, 3072], P('tp'), may hold values from -6 to 6
- gain_first: float32 [3072], replicated, may hold values from 0.1 to 1.9
- gain_second: float32 [3072], replicated, may hold values from 0.1 to 1.9
- gate_first: float32 [3072, 8192], P('fs', 'tp'), may hold values from -0.109375 to 0.109375
- up_first: float32 [3072, 8192], P('fs', 'tp'), may hold values from -0.109375 to 0.109375
- down_first: float32 [8192, 3072], P('fs', 'tp'), may hold values from -0.09375 to 0.09375
- gate_second: float32 [3072, 8192], P('fs', 'tp'), may hold values from -0.109375 to 0.109375
- up_second: float32 [3072, 8192], P('fs', 'tp'), may hold values from -0.109375 to 0.109375
- down_second: float32 [8192, 3072], P('fs', 'tp'), may hold values from -0.09375 to 0.09375
Outputs:
- result_rows: bfloat16 [640, 3072], P('tp')
- serve_gate_first: bfloat16 [3072, 8192], P(None, 'fs')
- serve_up_first: bfloat16 [3072, 8192], P(None, 'fs')
- serve_down_first: bfloat16 [8192, 3072], P('fs')
- serve_gate_second: bfloat16 [3072, 8192], P(None, 'fs')
- serve_up_second: bfloat16 [3072, 8192], P(None, 'fs')
- serve_down_second: bfloat16 [8192, 3072], P('fs')
All inputs are finite; a program needn't handle non-finite values.
Results may differ from a plain program's by a relative error of at most 0.011.
Values may be sent and summed in bfloat16 or wider, within the bound.
A program may use at most 192 MiB of HBM per device.

v0:
```python
import jax
import jax.numpy as jnp
from jax import lax
from jax.sharding import PartitionSpec as P


def plain_norm(values):
    values = values.astype(jnp.float32)
    center = jnp.mean(values, axis=-1, keepdims=True)
    spread = jnp.mean(jnp.square(values - center), axis=-1, keepdims=True)
    return (values - center) * lax.rsqrt(spread + 1e-05)


def sum_over_hidden(partial_value):
    pieces = lax.all_to_all(
        partial_value.astype(jnp.bfloat16), "fs", split_axis=1, concat_axis=0, tiled=True
    )
    rows = partial_value.shape[0]
    pieces = pieces.reshape(-1, rows, pieces.shape[1]).astype(jnp.float32)
    summed = jnp.sum(pieces, axis=0).astype(jnp.bfloat16)
    return lax.all_gather(summed, "fs", axis=1, tiled=True).astype(jnp.float32)


def regroup(folded):
    spread = lax.all_to_all(folded, "tp", split_axis=0, concat_axis=1, tiled=True)
    parts = lax.axis_size("fs")
    rows = spread.shape[0]
    owned = lax.all_to_all(spread, "fs", split_axis=1, concat_axis=0, tiled=True)
    owned = owned.reshape(parts, rows, owned.shape[1])
    whole = lax.all_gather(owned, "tp", axis=1, tiled=True)
    return whole.reshape(-1, whole.shape[2])


def half_step(normed, scales, w_gate, w_rising, w_down):
    gate_part = jnp.dot(normed, w_gate, preferred_element_type=jnp.float32)
    rising = jnp.dot(normed, w_rising, preferred_element_type=jnp.float32)
    hidden = (jax.nn.silu(gate_part) * rising).astype(jnp.bfloat16)
    partial_value = jnp.dot(hidden, w_down, preferred_element_type=jnp.float32)
    block = sum_over_hidden(partial_value)
    mixed = 1.6817928 * scales[None, :] * normed.astype(jnp.float32) + 0.5 * block
    return plain_norm(mixed).astype(jnp.bfloat16)


def on_device(
    tokens,
    gain_first,
    gain_second,
    gate_first,
    up_first,
    down_first,
    gate_second,
    up_second,
    down_second,
):
    row_count = gate_first.shape[0]
    offset = lax.axis_index("fs") * row_count

    def fold_gain(weight, scales):
        picked = lax.dynamic_slice_in_dim(scales, offset, row_count, 0)
        return (picked[:, None] * weight).astype(jnp.bfloat16)

    serve_gate_first = regroup(fold_gain(gate_first, gain_first))
    serve_up_first = regroup(fold_gain(up_first, gain_first))
    serve_down_first = lax.all_gather(
        down_first.astype(jnp.bfloat16), "tp", axis=1, tiled=True
    )
    serve_gate_second = regroup(fold_gain(gate_second, gain_second))
    serve_up_second = regroup(fold_gain(up_second, gain_second))
    serve_down_second = lax.all_gather(
        down_second.astype(jnp.bfloat16), "tp", axis=1, tiled=True
    )
    normed_zero = plain_norm(tokens).astype(jnp.bfloat16)
    normed_one = half_step(
        normed_zero, gain_first, serve_gate_first, serve_up_first, serve_down_first
    )
    result_rows = half_step(
        normed_one, gain_second, serve_gate_second, serve_up_second, serve_down_second
    )
    return (
        result_rows,
        serve_gate_first,
        serve_up_first,
        serve_down_first,
        serve_gate_second,
        serve_up_second,
        serve_down_second,
    )


def solution(mesh):
    placed = (
        P("tp", None),
        P(),
        P(),
        P("fs", "tp"),
        P("fs", "tp"),
        P("fs", "tp"),
        P("fs", "tp"),
        P("fs", "tp"),
        P("fs", "tp"),
    )
    return jax.shard_map(
        on_device,
        mesh=mesh,
        in_specs=placed,
        out_specs=(
            P("tp", None),
            P(None, "fs"),
            P(None, "fs"),
            P("fs", None),
            P(None, "fs"),
            P(None, "fs"),
            P("fs", None),
        ),
        check_vma=False,
    )
```

profile of v0, /device:TPU:0, one launch (start us, length us, event | category | flops | bytes accessed | tf_op | source)
XLA Modules:
  0.0 523.0 jit_solution(2696292961990616382)
XLA Ops:
  8.0 3.7 multiply_convert_fusion.3
  11.7 24.1 %all_to_all.154 = bf16[4,96,2048]{2,1,0:T(8,128)(2,1)S(1)} all-to-all(bf16[4,96,2048]{2,1,0:T(8,128)(2,1)S(1)} %bitcast.44), channel_id=1, replica_groups=mesh['fs'=8,'tp'=4] {'tp'}, dimensions={0} | all-to-all | bytes 3145728 | tf_op jit(solution)/shard_map/all_to_all | solution.py:25
  35.8 1.2 copy.28
  37.0 1.8 all_to_all.119
  38.9 2.3 copy.29
  41.2 42.3 %all_to_all.155 = bf16[96,8,1024]{2,0,1:T(8,128)(2,1)S(1)} all-to-all(bf16[96,8,1024]{2,0,1:T(8,128)(2,1)S(1)} %copy.29), channel_id=1, replica_groups=mesh['fs'=8,'tp'=4] {'fs'}, dimensions={1} | all-to-all | bytes 3145728 | tf_op jit(solution)/shard_map/all_to_all | solution.py:28
  83.5 2.0 copy.30
  85.6 36.1 %all_to_all.156 = bf16[4,96,2048]{2,1,0:T(8,128)(2,1)S(1)} all-to-all(bf16[4,96,2048]{2,1,0:T(8,128)(2,1)S(1)} %bitcast.42), channel_id=1, replica_groups=mesh['fs'=8,'tp'=4] {'tp'}, dimensions={0} | all-to-all | bytes 3145728 | tf_op jit(solution)/shard_map/all_to_all | solution.py:25
  121.7 1.2 copy.32
  123.3 0.9 copy.33
  124.2 39.1 %all_to_all.157 = bf16[96,8,1024]{2,0,1:T(8,128)(2,1)S(1)} all-to-all(bf16[96,8,1024]{2,0,1:T(8,128)(2,1)S(1)} %copy.33), channel_id=1, replica_groups=mesh['fs'=8,'tp'=4] {'fs'}, dimensions={1} | all-to-all | bytes 3145728 | tf_op jit(solution)/shard_map/all_to_all | solution.py:28
  163.3 2.0 copy.34
  165.4 1.3 convert_element_type.64
  166.8 3.9 multiply_convert_fusion.1
  170.7 39.8 %all_to_all.158 = bf16[4,96,2048]{2,1,0:T(8,128)(2,1)S(1)} all-to-all(bf16[4,96,2048]{2,1,0:T(8,128)(2,1)S(1)} %bitcast.45), channel_id=1, replica_groups=mesh['fs'=8,'tp'=4] {'tp'}, dimensions={0} | all-to-all | bytes 3145728 | tf_op jit(solution)/shard_map/all_to_all | solution.py:25
  210.5 1.2 copy.37
  211.7 1.8 all_to_all.133
  213.6 2.3 copy.38
  215.8 51.1 %all_to_all.159 = bf16[96,8,1024]{2,0,1:T(8,128)(2,1)S(1)} all-to-all(bf16[96,8,1024]{2,0,1:T(8,128)(2,1)S(1)} %copy.38), channel_id=1, replica_groups=mesh['fs'=8,'tp'=4] {'fs'}, dimensions={1} | all-to-all | bytes 3145728 | tf_op jit(solution)/shard_map/all_to_all | solution.py:28
  266.9 2.0 copy.39
  269.0 26.1 %all_to_all.160 = bf16[4,96,2048]{2,1,0:T(8,128)(2,1)S(1)} all-to-all(bf16[4,96,2048]{2,1,0:T(8,128)(2,1)S(1)} %bitcast.43), channel_id=1, replica_groups=mesh['fs'=8,'tp'=4] {'tp'}, dimensions={0} | all-to-all | bytes 3145728 | tf_op jit(solution)/shard_map/all_to_all | solution.py:25
  295.1 1.2 copy.41
  296.8 0.9 copy.42
  297.6 39.2 %all_to_all.161 = bf16[96,8,1024]{2,0,1:T(8,128)(2,1)S(1)} all-to-all(bf16[96,8,1024]{2,0,1:T(8,128)(2,1)S(1)} %copy.42), channel_id=1, replica_groups=mesh['fs'=8,'tp'=4] {'fs'}, dimensions={1} | all-to-all | bytes 3145728 | tf_op jit(solution)/shard_map/all_to_all | solution.py:28
  336.8 2.0 copy.43
  338.9 1.3 convert_element_type.72
  340.2 1.2 copy-done.1
  342.0 9.7 %copy.31 = bf16[8,384,1024]{2,1,0:T(8,128)(2,1)} copy(bf16[8,384,1024]{2,0,1:T(8,128)(2,1)} %all-gather.7.cloned.1.call-done) | data formatting | bytes 12582912 | tf_op jit(solution)/shard_map/all_gather | solution.py:30
  351.7 9.2 %copy.35 = bf16[8,384,1024]{2,1,0:T(8,128)(2,1)} copy(bf16[8,384,1024]{2,0,1:T(8,128)(2,1)} %all-gather.9.cloned.1.call-done) | data formatting | bytes 12582912 | tf_op jit(solution)/shard_map/all_gather | solution.py:30
  360.9 1.3 fusion.14
  362.3 7.0 %convolution_convert_fusion.1 = bf16[160,3072]{1,0:T(8,128)(2,1)S(1)} fusion(bf16[1024,3072]{1,0:T(8,128)(2,1)} %all-gather.11.cloned.1.call-done, bf16[3072,1024]{1,0:T(8,128)(2,1)} %bitcast.38, f32[160,1024]{1,0:T(8,128)S(1)} %fusion.14, bf16[160,3072]{1,0:T(8,128)(2,1)S(1)} %copy-done.1, f32[160]{0:T(256)S(1)} %add_rsqrt_fusion.2, ...), kind=kOutput, calls=%fused_computation.1 | convolution fusion | flops 2016706560 | bytes 15205632 | tf_op jit(solution)/shard_map/dot_general | solution.py:38
  369.3 1.0 copy.51
  370.3 3.8 all-to-all-start.4
  374.1 9.1 %copy.40 = bf16[8,384,1024]{2,1,0:T(8,128)(2,1)} copy(bf16[8,384,1024]{2,0,1:T(8,128)(2,1)} %all-gather.13.cloned.1.call-done) | data formatting | bytes 12582912 | tf_op jit(solution)/shard_map/all_gather | solution.py:30
  383.7 9.0 %copy.44 = bf16[8,384,1024]{2,1,0:T(8,128)(2,1)} copy(bf16[8,384,1024]{2,0,1:T(8,128)(2,1)} %all-gather.15.cloned.1.call-done) | data formatting | bytes 12582912 | tf_op jit(solution)/shard_map/all_gather | solution.py:30
  392.7 5.5 %all-to-all-done.4 = bf16[160,8,384]{2,0,1:T(8,128)(2,1)S(1)} async-done(((bf16[160,8,384]{2,0,1:T(8,128)(2,1)}), bf16[160,8,384]{2,0,1:T(8,128)(2,1)S(1)}, u32[]{:S(2)}, u32[]{:S(2)}) %all-to-all-start.4) | async-done | bytes 983072 | tf_op jit(solution)/shard_map/all_to_all | solution.py:15
  398.3 33.7 %all_gather.27 = bf16[160,3072]{1,0:T(8,128)(2,1)S(1)} all-gather(bf16[160,384]{1,0:T(8,128)(2,1)S(1)} %reduce_sum.80), channel_id=1, replica_groups=mesh['fs'=8,'tp'=4] {'fs'}, dimensions={1}, use_global_device_ids=true | all-gather | bytes 1105920 | tf_op jit(solution)/shard_map/all_gather | solution.py:21
  432.6 0.8 multiply_reduce_fusion.1
  433.4 0.9 multiply_convert_fusion.5
  434.7 1.3 fusion.16
  436.0 6.9 %convolution_convert_fusion = bf16[160,3072]{1,0:T(8,128)(2,1)S(1)} fusion(bf16[1024,3072]{1,0:T(8,128)(2,1)} %all-gather.17.cloned.1.call-done, bf16[160,3072]{1,0:T(8,128)(2,1)S(1)} %multiply_convert_fusion.5, bf16[3072,1024]{1,0:T(8,128)(2,1)} %bitcast.40, f32[160,1024]{1,0:T(8,128)S(1)} %fusion.16), kind=kOutput, calls=%fused_computation | convolution fusion | flops 2014740480 | bytes 15204352 | tf_op jit(solution)/shard_map/dot_general | solution.py:38
  442.9 1.0 copy.50
  444.0 3.6 all-to-all-start.9
  447.6 23.0 %all-to-all-done.9 = bf16[160,8,384]{2,0,1:T(8,128)(2,1)S(1)} async-done(((bf16[160,8,384]{2,0,1:T(8,128)(2,1)}), bf16[160,8,384]{2,0,1:T(8,128)(2,1)S(1)}, u32[]{:S(2)}, u32[]{:S(2)}) %all-to-all-start.9) | async-done | bytes 983072 | tf_op jit(solution)/shard_map/all_to_all | solution.py:15
  470.6 33.6 %all_gather.31 = bf16[160,3072]{1,0:T(8,128)(2,1)S(1)} all-gather(bf16[160,384]{1,0:T(8,128)(2,1)S(1)} %reduce_sum.83), channel_id=1, replica_groups=mesh['fs'=8,'tp'=4] {'fs'}, dimensions={1}, use_global_device_ids=true | all-gather | bytes 1105920 | tf_op jit(solution)/shard_map/all_gather | solution.py:21
  505.4 1.5 multiply_convert_fusion.4
  506.9 6.1 %copy.54 = bf16[1024,3072]{1,0:T(8,128)(2,1)} copy(bf16[1024,3072]{1,0:T(8,128)(2,1)} %all-gather.11.cloned.1.call-done) | data formatting | bytes 12582912
  513.0 2.7 copy.55
  (55 shorter events, 5.7 us)
Async XLA Ops:
  7.2 334.9 %all-gather.7.cloned.1.call-start = ((), (), s32[]{:S(2)}) async-start(), calls=%async_computation.10 | async-start | bytes 7864320 | tf_op jit(solution)/shard_map/all_gather | solution.py:30
  85.5 266.2 %all-gather.9.cloned.1.call-start = ((), (), s32[]{:S(2)}) async-start(), calls=%async_computation.11 | async-start | bytes 7864320 | tf_op jit(solution)/shard_map/all_gather | solution.py:30
  163.3 2.1 copy-start.3
  165.3 1.4 copy-start.6
  165.3 196.9 %all-gather.11.cloned.1.call-start = ((), (), s32[]{:S(2)}) async-start(), calls=%async_computation.12 | async-start | bytes 7864320 | tf_op jit(solution)/shard_map/all_gather | solution.py:64
  166.7 207.4 %all-gather.13.cloned.1.call-start = ((), (), s32[]{:S(2)}) async-start(), calls=%async_computation.13 | async-start | bytes 7864320 | tf_op jit(solution)/shard_map/all_gather | solution.py:30
  269.0 114.7 %all-gather.15.cloned.1.call-start = ((), (), s32[]{:S(2)}) async-start(), calls=%async_computation.14 | async-start | bytes 7864320 | tf_op jit(solution)/shard_map/all_gather | solution.py:30
  336.8 2.1 copy-start.4
  338.8 97.2 %all-gather.17.cloned.1.call-start = ((), (), s32[]{:S(2)}) async-start(), calls=%async_computation.15 | async-start | bytes 7864320 | tf_op jit(solution)/shard_map/all_gather | solution.py:69
  340.2 1.2 copy-start.1
  351.7 9.2 %copy-start.2 = (bf16[8,384,1024]{2,1,0:T(8,128)(2,1)S(1)}, bf16[8,384,1024]{2,1,0:T(8,128)(2,1)}, u32[]{:S(2)}) copy-start(bf16[8,384,1024]{2,1,0:T(8,128)(2,1)} %copy.31) | copy-start | bytes 18874372
  369.3 4.8 copy-start.5
  370.3 27.8 %all-to-all-start.4 = ((bf16[160,8,384]{2,0,1:T(8,128)(2,1)}), bf16[160,8,384]{2,0,1:T(8,128)(2,1)S(1)}, u32[]{:S(2)}, u32[]{:S(2)}) async-start(bf16[160,8,384]{2,0,1:T(8,128)(2,1)} %bitcast.31), calls=%async_computation.4 | async-start | bytes 1966080 | tf_op jit(solution)/shard_map/all_to_all | solution.py:15
  432.0 2.8 copy-start
  444.0 26.5 %all-to-all-start.9 = ((bf16[160,8,384]{2,0,1:T(8,128)(2,1)}), bf16[160,8,384]{2,0,1:T(8,128)(2,1)S(1)}, u32[]{:S(2)}, u32[]{:S(2)}) async-start(bf16[160,8,384]{2,0,1:T(8,128)(2,1)} %bitcast.30), calls=%async_computation.9 | async-start | bytes 1966080 | tf_op jit(solution)/shard_map/all_to_all | solution.py:15
  505.4 7.6 %slice-start = ((s8[6291456]{0:T(1024)(128)(4,1)}), s8[4194304]{0:T(1024)(128)(4,1)S(1)}, s32[]{:S(2)}) async-start(s8[6291456]{0:T(1024)(128)(4,1)} %bitcast.34), calls=%async_computation.16 | async-start | bytes 8388608
  506.9 6.1 %slice-start.1 = ((s8[6291456]{0:T(1024)(128)(4,1)}), s8[2097152]{0:T(1024)(128)(4,1)S(1)}, s32[]{:S(2)}) async-start(s8[6291456]{0:T(1024)(128)(4,1)} %bitcast.34), calls=%async_computation.17 | async-start | bytes 4194304
Sparse Core Ops, SparseCore 0:
  85.6 57.7 all-gather.6
  165.4 61.2 all-gather.8
  228.8 46.1 all-gather.10
  276.5 50.4 all-gather.12
  338.9 44.6 all-gather.14
  385.7 46.3 all-gather.16
where the time goes:
time: 531 us; the launch traced here: 523 us
  blocking collectives  365 us (69%)
  local copies, waits for them, and re-layouts  74 us (14%)
  waiting for transfers between devices  29.1 us (5%)
  matrix products  16.4 us (3%)
  other arithmetic  16.1 us (3%)
  between operations  14.8 us (3%)
  starting transfers between devices  7.57 us (1%)
    all_to_all x4, blocking collectives, regroup(): lax.all_to_all(spread, 'fs', split_axis=1, concat_axis=0, tiled=True)  172 us
    all_to_all x4, blocking collectives, regroup(): lax.all_to_all(folded, 'tp', split_axis=0, concat_axis=1, tiled=True)  126 us
    all_gather x2, blocking collectives, sum_over_hidden(): return lax.all_gather(summed, 'fs', axis=1, tiled=True).astype(jnp.float32)  67.3 us
    all_gather x4, local copies, waits for them, and re-layouts, regroup(): whole = lax.all_gather(owned, 'tp', axis=1, tiled=True)  36.9 us
    all_to_all x2, waiting for transfers between devices, sum_over_hidden(): lax.all_to_all(partial_value.astype(jnp.bfloat16), 'fs', split_axis=1, co...  28.4 us
    all_to_all x12, local copies, waits for them, and re-layouts, regroup(): lax.all_to_all(spread, 'fs', split_axis=1, concat_axis=0, tiled=True)  18.8 us
    dot_general x2, matrix products, half_step(): partial_value = jnp.dot(hidden, w_down, preferred_element_type=jnp.float32)  13.9 us
  transfers between devices with their start and end apart: 8, of which 3 were waited for; matrix products, arithmetic and copies ran while one was open for 14% of the time, Pallas kernels for 0%

commit v1 on v0

v1 whole, which is shorter than its diff:
```python
import functools

import jax
import jax.numpy as jnp
from jax import lax
from jax.experimental import pallas as pl
from jax.experimental.pallas import tpu as pltpu
from jax.sharding import PartitionSpec as P

MESH = pl.DeviceIdType.MESH
CORES = 2
SIDES = 2
RELAY = 6


def plain_norm(values):
    values = values.astype(jnp.float32)
    center = jnp.mean(values, axis=-1, keepdims=True)
    spread = jnp.mean(jnp.square(values - center), axis=-1, keepdims=True)
    return (values - center) * lax.rsqrt(spread + 1e-05)


def sum_over_hidden(partial_value):
    pieces = lax.all_to_all(
        partial_value.astype(jnp.bfloat16), "fs", split_axis=1, concat_axis=0, tiled=True
    )
    rows = partial_value.shape[0]
    pieces = pieces.reshape(-1, rows, pieces.shape[1]).astype(jnp.float32)
    summed = jnp.sum(pieces, axis=0).astype(jnp.bfloat16)
    return lax.all_gather(summed, "fs", axis=1, tiled=True).astype(jnp.float32)


def regroup(folded):
    spread = lax.all_to_all(folded, "tp", split_axis=0, concat_axis=1, tiled=True)
    parts = lax.axis_size("fs")
    rows = spread.shape[0]
    owned = lax.all_to_all(spread, "fs", split_axis=1, concat_axis=0, tiled=True)
    owned = owned.reshape(parts, rows, owned.shape[1])
    whole = lax.all_gather(owned, "tp", axis=1, tiled=True)
    return whole.reshape(-1, whole.shape[2])


def collect_plain(gate, up, down):
    return (
        regroup(gate),
        regroup(up),
        lax.all_gather(down, "tp", axis=1, tiled=True),
    )


def close_plain(partial_value, normed, scales):
    block = sum_over_hidden(partial_value)
    mixed = 1.6817928 * scales[None, :] * normed.astype(jnp.float32) + 0.5 * block
    return plain_norm(mixed).astype(jnp.bfloat16)


class Send:
    def __init__(self, when, src, dst, send, recv, to):
        self.when = when
        self.copy = pltpu.make_async_remote_copy(
            src_ref=src,
            dst_ref=dst,
            send_sem=send,
            recv_sem=recv,
            device_id=to,
            device_id_type=MESH,
        )

    def start(self):
        if self.when is None:
            self.copy.start()
        else:
            pl.when(self.when)(self.copy.start)

    def wait_send(self):
        if self.when is None:
            self.copy.wait_send()
        else:
            pl.when(self.when)(self.copy.wait_send)


def landed(ref, sem):
    pltpu.make_async_copy(ref, ref, sem).wait()


def collect_kernel(
    gate,
    up,
    down,
    whole_gate,
    whole_up,
    whole_down,
    passing,
    bounce,
    bounce_down,
    s_plane,
    s_cross,
    r_cross,
    s_pass,
    r_main,
    r_minor,
    s_main,
    s_minor,
    s_over,
    s_down,
    r_down,
    l_own,
    l_down,
):
    fs = lax.axis_index("fs")
    tp = lax.axis_index("tp")
    z, y = fs // SIDES, fs % SIDES
    x, c = tp // CORES, tp % CORES
    half = z // 2
    aligned = x == half
    primary = c == z % 2
    rows = gate.shape[0]
    width = whole_gate.shape[1]
    part = rows // RELAY
    main = rows - part
    here = lambda col: (fs, col)
    peer = (1 - x) * CORES + c
    sibling = x * CORES + 1 - c
    across = (1 - x) * CORES + 1 - c
    sources = (gate, up)
    targets = (whole_gate, whole_up)
    started = []

    def send(*args):
        one = Send(*args)
        one.start()
        started.append(one)

    def cols(ref, start, size, side):
        return ref.at[pl.ds(start, size), pl.ds(side * width, width)]

    def at(ref, owner, start, size):
        first = pl.multiple_of(owner * rows + start, 16)
        return ref.at[pl.ds(first, size), :]

    main_at = jnp.where(aligned, part, 0)
    over_at = jnp.where(aligned, main, 0)
    minor_at = jnp.where(aligned, 0, main)

    zone = x * CORES + c
    for m in range(2):
        for side in range(SIDES):
            owner = zone * SIDES + side
            unaligned = jnp.logical_not(aligned)
            send(
                unaligned,
                cols(sources[m], 0, main, side),
                passing.at[m, side],
                s_cross.at[m, side],
                r_cross.at[m, side],
                here(peer),
            )
            send(
                unaligned,
                cols(sources[m], part, main, side),
                at(targets[m], fs, part, main),
                s_plane.at[m, side],
                r_main.at[m, fs],
                (owner, tp),
            )
            send(
                jnp.logical_and(aligned, owner != fs),
                cols(sources[m], 0, rows, side),
                at(targets[m], fs, 0, rows),
                s_plane.at[m, side],
                r_main.at[m, fs],
                (owner, tp),
            )

    lanes = down.shape[1]

    def column(ref, col):
        return ref.at[:, pl.ds(pl.multiple_of(col * lanes, 128), lanes)]

    send(None, down, column(whole_down, tp), s_down.at[0], r_down.at[0], here(peer))
    send(None, down, column(whole_down, tp), s_down.at[1], r_down.at[1], here(sibling))

    home = jnp.logical_and(aligned, primary)

    def own(ref):
        return ref.at[:, pl.ds(pl.multiple_of(y * width, 128), width)]

    for m in range(2):
        send(
            home,
            own(sources[m]),
            at(targets[m], fs, 0, rows),
            s_over.at[m, fs],
            r_main.at[m, fs],
            here(peer),
        )
        send(
            home,
            own(sources[m]),
            at(targets[m], fs, 0, rows),
            s_main.at[m, fs],
            r_main.at[m, fs],
            here(sibling),
        )

    to_bounce = pltpu.make_async_copy(down, bounce_down, l_down)
    to_bounce.start()
    for m in range(2):
        fetch = pltpu.make_async_copy(own(sources[m]), bounce.at[m], l_own.at[m])
        pl.when(home)(fetch.start)
    to_bounce.wait()
    put_down = pltpu.make_async_copy(bounce_down, column(whole_down, tp), l_down)
    put_down.start()
    puts = []
    for m in range(2):
        fetch = pltpu.make_async_copy(own(sources[m]), bounce.at[m], l_own.at[m])
        put = pltpu.make_async_copy(
            bounce.at[m], at(targets[m], fs, 0, rows), l_own.at[m]
        )
        puts.append(put)
        pl.when(home)(fetch.wait)
        pl.when(home)(put.start)

    far_zone = (1 - x) * CORES + c
    for m in range(2):
        for side in range(SIDES):
            pl.when(aligned)(
                functools.partial(landed, passing.at[m, side], r_cross.at[m, side])
            )
            send(
                aligned,
                passing.at[m, side],
                at(targets[m], fs, 0, main),
                s_pass.at[m, side],
                r_main.at[m, fs],
                (far_zone * SIDES + side, tp),
            )

    for m in range(2):
        for step in range(2 * SIDES):
            owner = half * 2 * SIDES + (fs + step) % (2 * SIDES)
            is_home = owner == fs
            block = at(targets[m], owner, 0, rows)
            if step == 0:
                got = jnp.logical_and(primary, jnp.logical_not(aligned))
            else:
                got = primary
            pl.when(got)(functools.partial(landed, block, r_main.at[m, owner]))
            send(
                got,
                block,
                block,
                s_main.at[m, owner],
                r_main.at[m, owner],
                here(sibling),
            )
            if step:
                send(
                    jnp.logical_and(primary, aligned),
                    block,
                    block,
                    s_over.at[m, owner],
                    r_main.at[m, owner],
                    here(peer),
                )

    landed(column(whole_down, peer), r_down.at[0])
    send(
        None,
        column(whole_down, peer),
        column(whole_down, peer),
        s_down.at[2],
        r_down.at[2],
        here(sibling),
    )

    for m in range(2):
        for step in range(2 * SIDES):
            owner = (1 - half) * 2 * SIDES + (fs + step) % (2 * SIDES)
            block = at(targets[m], owner, main_at, main)
            over = at(targets[m], owner, over_at, part)
            pl.when(primary)(functools.partial(landed, block, r_main.at[m, owner]))
            send(
                primary,
                over,
                over,
                s_over.at[m, owner],
                r_minor.at[m, owner],
                here(peer),
            )
            send(
                primary,
                block,
                block,
                s_main.at[m, owner],
                r_main.at[m, owner],
                here(sibling),
            )
    for m in range(2):
        for step in range(2 * SIDES):
            owner = (1 - half) * 2 * SIDES + (fs + step) % (2 * SIDES)
            block = at(targets[m], owner, minor_at, part)
            pl.when(primary)(functools.partial(landed, block, r_minor.at[m, owner]))
            send(
                primary,
                block,
                block,
                s_minor.at[m, owner],
                r_minor.at[m, owner],
                here(sibling),
            )

    second = jnp.logical_not(primary)
    for m in range(2):
        for step in range(2 * SIDES):
            owner = half * 2 * SIDES + (fs + step) % (2 * SIDES)
            pl.when(second)(
                functools.partial(
                    landed, at(targets[m], owner, 0, rows), r_main.at[m, owner]
                )
            )
            owner = (1 - half) * 2 * SIDES + (fs + step) % (2 * SIDES)
            pl.when(second)(
                functools.partial(
                    landed, at(targets[m], owner, main_at, main), r_main.at[m, owner]
                )
            )
            pl.when(second)(
                functools.partial(
                    landed, at(targets[m], owner, minor_at, part), r_minor.at[m, owner]
                )
            )
    landed(column(whole_down, sibling), r_down.at[1])
    landed(column(whole_down, across), r_down.at[2])
    put_down.wait()
    for put in puts:
        pl.when(home)(put.wait)
    for one in started:
        one.wait_send()


def collect(gate, up, down):
    rows, columns = gate.shape
    fs, tp = lax.axis_size("fs"), lax.axis_size("tp")
    width = columns * tp // fs
    main = rows - rows // RELAY
    grid_like = jax.ShapeDtypeStruct((rows * fs, width), jnp.bfloat16)
    any_place = pl.BlockSpec(memory_space=pl.ANY)
    dma = pltpu.SemaphoreType.DMA
    return pl.pallas_call(
        collect_kernel,
        out_shape=(
            grid_like,
            grid_like,
            jax.ShapeDtypeStruct((down.shape[0], down.shape[1] * tp), jnp.bfloat16),
        ),
        in_specs=[any_place] * 3,
        out_specs=(any_place,) * 3,
        scratch_shapes=[
            pltpu.VMEM((2, SIDES, main, width), jnp.bfloat16),
            pltpu.VMEM((2, rows, width), jnp.bfloat16),
            pltpu.VMEM(down.shape, jnp.bfloat16),
            dma((2, SIDES)),
            dma((2, SIDES)),
            dma((2, SIDES)),
            dma((2, SIDES)),
            dma((2, fs)),
            dma((2, fs)),
            dma((2, fs)),
            dma((2, fs)),
            dma((2, fs)),
            dma((3,)),
            dma((3,)),
            dma((2,)),
            dma(()),
        ],
        compiler_params=pltpu.CompilerParams(has_side_effects=True),
    )(gate, up, down)


def close_kernel(
    partial_value, normed, scales, out, landing, summed, full, s_part, r_part, s_sum, r_sum
):
    fs = lax.axis_index("fs")
    tp = lax.axis_index("tp")
    count = lax.axis_size("fs")
    rows, width = summed.shape

    def lanes(index):
        return pl.ds(pl.multiple_of(index * width, 128), width)

    copies = []
    for step in range(1, count):
        to = (fs + step) % count
        copy = pltpu.make_async_remote_copy(
            src_ref=partial_value.at[:, lanes(to)],
            dst_ref=landing.at[step - 1],
            send_sem=s_part.at[step - 1],
            recv_sem=r_part.at[step - 1],
            device_id=(to, tp),
            device_id_type=MESH,
        )
        copy.start()
        copies.append(copy)
    for copy in copies:
        copy.wait_recv()
    total = partial_value[:, lanes(fs)].astype(jnp.float32)
    for step in range(1, count):
        total += landing[step - 1].astype(jnp.float32)
    summed[...] = total.astype(jnp.bfloat16)
    sums = []
    for step in range(1, count):
        to = (fs + step) % count
        copy = pltpu.make_async_remote_copy(
            src_ref=summed,
            dst_ref=full.at[fs],
            send_sem=s_sum.at[step - 1],
            recv_sem=r_sum.at[step - 1],
            device_id=(to, tp),
            device_id_type=MESH,
        )
        copy.start()
        sums.append(copy)
    full[fs] = summed[...]
    for copy in sums:
        copy.wait_recv()
    step = 16

    def norm(index, carry):
        some = pl.ds(pl.multiple_of(index * step, step), step)
        block = jnp.concatenate(
            [full[k, some, :].astype(jnp.float32) for k in range(count)], axis=1
        )
        mixed = 1.6817928 * scales[...] * normed[some, :].astype(jnp.float32) + 0.5 * block
        out[some, :] = plain_norm(mixed).astype(jnp.bfloat16)
        return carry

    lax.fori_loop(0, rows // step, norm, 0)
    for copy in copies + sums:
        copy.wait_send()


def close(partial_value, normed, scales):
    rows, width = normed.shape
    count = lax.axis_size("fs")
    piece = width // count
    vmem = pl.BlockSpec(memory_space=pltpu.VMEM)
    dma = pltpu.SemaphoreType.DMA
    return pl.pallas_call(
        close_kernel,
        out_shape=jax.ShapeDtypeStruct((rows, width), jnp.bfloat16),
        in_specs=[vmem] * 3,
        out_specs=vmem,
        scratch_shapes=[
            pltpu.VMEM((count - 1, rows, piece), jnp.bfloat16),
            pltpu.VMEM((rows, piece), jnp.bfloat16),
            pltpu.VMEM((count, rows, piece), jnp.bfloat16),
            dma((count - 1,)),
            dma((count - 1,)),
            dma((count - 1,)),
            dma((count - 1,)),
        ],
        compiler_params=pltpu.CompilerParams(has_side_effects=True),
    )(partial_value.astype(jnp.bfloat16), normed, scales[None, :])


def on_device(
    use_kernels,
    tokens,
    gain_first,
    gain_second,
    gate_first,
    up_first,
    down_first,
    gate_second,
    up_second,
    down_second,
):
    row_count = gate_first.shape[0]
    offset = lax.axis_index("fs") * row_count
    bring = collect if use_kernels else collect_plain
    finish = close if use_kernels else close_plain

    def fold_gain(weight, scales):
        picked = lax.dynamic_slice_in_dim(scales, offset, row_count, 0)
        return (picked[:, None] * weight).astype(jnp.bfloat16)

    def half_step(normed, scales, w_gate, w_rising, w_down):
        gate_part = jnp.dot(normed, w_gate, preferred_element_type=jnp.float32)
        rising = jnp.dot(normed, w_rising, preferred_element_type=jnp.float32)
        hidden = (jax.nn.silu(gate_part) * rising).astype(jnp.bfloat16)
        partial_value = jnp.dot(hidden, w_down, preferred_element_type=jnp.float32)
        return finish(partial_value, normed, scales)

    first = bring(
        fold_gain(gate_first, gain_first),
        fold_gain(up_first, gain_first),
        down_first.astype(jnp.bfloat16),
    )
    second = bring(
        fold_gain(gate_second, gain_second),
        fold_gain(up_second, gain_second),
        down_second.astype(jnp.bfloat16),
    )
    normed_zero = plain_norm(tokens).astype(jnp.bfloat16)
    normed_one = half_step(normed_zero, gain_first, *first)
    result_rows = half_step(normed_one, gain_second, *second)
    return (result_rows, *first, *second)


def solution(mesh):
    fs, tp = mesh.shape["fs"], mesh.shape["tp"]
    use_kernels = tp == 2 * CORES and fs == tp * SIDES
    placed = (P("tp", None), P(), P()) + (P("fs", "tp"),) * 6
    served = (P(None, "fs"), P(None, "fs"), P("fs", None))
    return jax.shard_map(
        functools.partial(on_device, use_kernels),
        mesh=mesh,
        in_specs=placed,
        out_specs=(P("tp", None),) + served + served,
        check_vma=False,
    )
```

time: 531 us -> 472 us (0.89)
  Pallas kernels: 0 us -> 399 us
  blocking collectives: 365 us -> 0 us
  local copies, waits for them, and re-layouts: 74 us -> 30.2 us
  waiting for transfers between devices: 29.1 us -> 0 us
  between operations: 14.8 us -> 0.77 us
  matrix products: 16.4 us -> 24 us
  starting transfers between devices: 7.57 us -> 0 us
    pallas_call x0 -> x4, Pallas kernels: none -> 399 us  [the longest x2 277 us: collect(): pl.pallas_call(collect_kernel, out_shape=(grid_like, grid_like, jax.Shape...]
    all_to_all x8 -> x0, blocking collectives: 298 us -> none  [the longest x4 172 us: regroup(): lax.all_to_all(spread, 'fs', split_axis=1, concat_axis=0, tiled=True)]
    all_gather x2 -> x0, blocking collectives: 67.3 us -> none  [sum_over_hidden(): return lax.all_gather(summed, 'fs', axis=1, tiled=True).astype(jnp.float32)]
    all_gather x4 -> x0, local copies, waits for them, and re-layouts: 36.9 us -> none  [regroup(): whole = lax.all_gather(owned, 'tp', axis=1, tiled=True)]
    all_to_all x2 -> x0, waiting for transfers between devices: 28.4 us -> none  [sum_over_hidden(): lax.all_to_all(partial_value.astype(jnp.bfloat16), 'fs', split_axis=1, co...]
    all_to_all x18 -> x0, local copies, waits for them, and re-layouts: 25.8 us -> none  [the longest x12 18.8 us: regroup(): lax.all_to_all(spread, 'fs', split_axis=1, concat_axis=0, tiled=True)]
    unnamed x20 -> x37, local copies, waits for them, and re-layouts: 10.4 us -> 28.6 us
    all_to_all x2 -> x0, starting transfers between devices: 7.32 us -> none  [sum_over_hidden(): lax.all_to_all(partial_value.astype(jnp.bfloat16), 'fs', split_axis=1, co...]
  transfers between devices with their start and end apart: 8 -> 0, of which waited for: 3 -> 0; matrix products, arithmetic and copies ran while one was open for 14% -> 0% of each run, Pallas kernels for 0% -> 0%
where the time goes in v1:
time: 472 us; the launch traced here: 469 us
  Pallas kernels  399 us (85%)
  local copies, waits for them, and re-layouts  30.2 us (6%)
  matrix products  24 us (5%)
  other arithmetic  14.9 us (3%)
    pallas_call x2, Pallas kernels, collect(): pl.pallas_call(collect_kernel, out_shape=(grid_like, grid_like, jax.Shape...  277 us
    pallas_call x2, Pallas kernels, close(): pl.pallas_call(close_kernel, out_shape=jax.ShapeDtypeStruct((rows, width)...  123 us
    unnamed x37, local copies, waits for them, and re-layouts  28.6 us
    dot_general x2, matrix products, half_step(): partial_value = jnp.dot(hidden, w_down, preferred_element_type=jnp.float32)  15.7 us
    convert_element_type x2, other arithmetic, fold_gain(): return (picked[:, None] * weight).astype(jnp.bfloat16)  11.3 us

profile of v1, /device:TPU:0, one launch (start us, length us, event | category | flops | bytes accessed | tf_op | source)
XLA Modules:
  0.0 468.9 jit_solution(9459542382811445332)
XLA Ops:
  0.6 0.8 dynamic_slice.8
  1.4 0.0 copy-start.3
  1.4 5.6 %multiply_convert_fusion.2 = (bf16[384,2048]{1,0:T(8,128)(2,1)}, bf16[384,2048]{1,0:T(8,128)(2,1)}) fusion(f32[384,2048]{1,0:T(8,128)} %param.13, f32[384]{0:T(512)S(1)} %dynamic_slice.8, f32[384,2048]{1,0:T(8,128)} %param.12), kind=kLoop, calls=%fused_computation.4 | loop fusion | flops 3145728 | bytes 9438720 | tf_op jit(solution)/shard_map/convert_element_type | solution.py:486
  7.0 0.0 copy-done.3
  7.0 1.3 convert_element_type.40.down
  8.3 0.0 copy-start
  8.3 137.0 %shard_map.144 = (bf16[3072,1024]{1,0:T(8,128)(2,1)}, bf16[3072,1024]{1,0:T(8,128)(2,1)}, bf16[1024,3072]{1,0:T(8,128)(2,1)}) custom-call(bf16[384,2048]{1,0:T(8,128)(2,1)} %get-tuple-element.20.gate, bf16[384,2048]{1,0:T(8,128)(2,1)} %get-tuple-element.19.up, bf16[1024,768]{1,0:T(8,128)(2,1)} %convert_element_type.40.down), custom_call_target="tpu_custom_call" | custom-call | tf_op jit(solution)/shard_map/pallas_call | solution.py:350
  145.4 0.0 copy-done
  145.4 0.2 convert_reduce_fusion
  145.6 0.4 fusion.2
  146.0 0.4 fusion.3.normed
  146.4 0.0 copy-start.2
  146.4 4.3 fusion.10
  150.7 0.0 copy-done.2
  150.7 7.8 %convolution_convert_fusion.1.partial_value = bf16[160,3072]{1,0:T(8,128)(2,1)} fusion(bf16[1024,3072]{1,0:T(8,128)(2,1)} %get-tuple-element.33, bf16[160,3072]{1,0:T(8,128)(2,1)S(1)} %fusion.3.normed, bf16[3072,1024]{1,0:T(8,128)(2,1)} %get-tuple-element.32, f32[160,1024]{1,0:T(8,128)S(1)} %fusion.10), kind=kOutput, calls=%fused_computation.1 | convolution fusion | flops 2014740480 | bytes 15204352 | tf_op jit(solution)/shard_map/dot_general | solution.py:492
  158.6 61.3 %shard_map.145.normed = bf16[160,3072]{1,0:T(8,128)(2,1)} custom-call(bf16[160,3072]{1,0:T(8,128)(2,1)} %convolution_convert_fusion.1.partial_value, bf16[160,3072]{1,0:T(8,128)(2,1)} %copy-done.2, f32[1,3072]{1,0:T(1,128)} %bitcast.22), custom_call_target="tpu_custom_call" | custom-call | tf_op jit(solution)/shard_map/pallas_call | solution.py:449
  219.9 0.8 dynamic_slice.9
  220.7 0.0 copy-start.4
  220.7 5.6 %multiply_convert_fusion = (bf16[384,2048]{1,0:T(8,128)(2,1)}, bf16[384,2048]{1,0:T(8,128)(2,1)}) fusion(f32[384,2048]{1,0:T(8,128)} %param.16, f32[384]{0:T(512)S(1)} %dynamic_slice.9, f32[384,2048]{1,0:T(8,128)} %param.15), kind=kLoop, calls=%fused_computation.2 | loop fusion | flops 3145728 | bytes 9438720 | tf_op jit(solution)/shard_map/convert_element_type | solution.py:486
  226.3 0.0 copy-done.4
  226.3 1.3 convert_element_type.45.down
  227.6 0.0 copy-start.1
  227.6 139.5 %shard_map.146 = (bf16[3072,1024]{1,0:T(8,128)(2,1)}, bf16[3072,1024]{1,0:T(8,128)(2,1)}, bf16[1024,3072]{1,0:T(8,128)(2,1)}) custom-call(bf16[384,2048]{1,0:T(8,128)(2,1)} %get-tuple-element.22.gate, bf16[384,2048]{1,0:T(8,128)(2,1)} %get-tuple-element.21.up, bf16[1024,768]{1,0:T(8,128)(2,1)} %convert_element_type.45.down), custom_call_target="tpu_custom_call" | custom-call | tf_op jit(solution)/shard_map/pallas_call | solution.py:350
  367.1 0.0 copy-done.1
  367.2 4.0 fusion.11
  371.1 7.8 %convolution_convert_fusion.partial_value = bf16[160,3072]{1,0:T(8,128)(2,1)} fusion(bf16[1024,3072]{1,0:T(8,128)(2,1)} %get-tuple-element.36, bf16[160,3072]{1,0:T(8,128)(2,1)S(1)} %copy-done.1, bf16[3072,1024]{1,0:T(8,128)(2,1)} %get-tuple-element.35, f32[160,1024]{1,0:T(8,128)S(1)} %fusion.11), kind=kOutput, calls=%fused_computation | convolution fusion | flops 2014740480 | bytes 15204352 | tf_op jit(solution)/shard_map/dot_general | solution.py:492
  379.0 0.0 slice-start.4
  379.0 61.3 %shard_map.147 = bf16[160,3072]{1,0:T(8,128)(2,1)} custom-call(bf16[160,3072]{1,0:T(8,128)(2,1)} %convolution_convert_fusion.partial_value, bf16[160,3072]{1,0:T(8,128)(2,1)} %shard_map.145.normed, f32[1,3072]{1,0:T(1,128)} %bitcast.23), custom_call_target="tpu_custom_call" | custom-call | tf_op jit(solution)/shard_map/pallas_call | solution.py:449
  440.3 2.2 copy.23
  442.5 0.0 slice-start.5
  442.5 6.5 %copy.24 = bf16[3072,1024]{1,0:T(8,128)(2,1)} copy(bf16[3072,1024]{1,0:T(8,128)(2,1)} %get-tuple-element.31) | data formatting | bytes 12582912
  448.9 0.0 slice-done.4
  448.9 0.0 slice-done.5
  448.9 0.0 slice-start
  449.0 3.2 copy.25
  452.2 0.0 slice-done.2
  452.2 0.0 slice-done.3
  452.2 0.0 slice-start.8
  452.2 3.2 copy.26
  455.4 0.7 slice-done
  456.1 0.9 slice-done.1
  457.0 3.2 copy.27
  460.1 0.0 slice-done.8
  460.2 1.4 slice-done.9
  461.6 3.2 copy.28
  464.8 0.0 slice-done.6
  464.8 1.4 slice-done.7
  466.2 2.7 copy.29
  (13 shorter events, 0.0 us)
Async XLA Ops:
  1.4 5.6 %copy-start.3 = (f32[1024,768]{1,0:T(8,128)S(1)}, f32[1024,768]{1,0:T(8,128)}, u32[]{:S(2)}) copy-start(f32[1024,768]{1,0:T(8,128)} %param.14) | copy-start | bytes 9437188
  8.3 137.0 %copy-start = (bf16[160,3072]{1,0:T(8,128)(2,1)S(1)}, bf16[160,3072]{1,0:T(8,128)(2,1)}, u32[]{:S(2)}) copy-start(bf16[160,3072]{1,0:T(8,128)(2,1)} %param.9) | copy-start | bytes 2949124
  146.4 4.3 copy-start.2
  220.7 5.6 %copy-start.4 = (f32[1024,768]{1,0:T(8,128)S(1)}, f32[1024,768]{1,0:T(8,128)}, u32[]{:S(2)}) copy-start(f32[1024,768]{1,0:T(8,128)} %param.17) | copy-start | bytes 9437188
  227.6 139.5 %copy-start.1 = (bf16[160,3072]{1,0:T(8,128)(2,1)S(1)}, bf16[160,3072]{1,0:T(8,128)(2,1)}, u32[]{:S(2)}) copy-start(bf16[160,3072]{1,0:T(8,128)(2,1)} %shard_map.145.normed) | copy-start | bytes 2949124
  379.0 70.0 %slice-start.4 = ((s8[6291456]{0:T(1024)(128)(4,1)}), s8[2097152]{0:T(1024)(128)(4,1)S(1)}, s32[]{:S(2)}) async-start(s8[6291456]{0:T(1024)(128)(4,1)} %bitcast.16), calls=%async_computation.4 | async-start | bytes 4194304
  442.5 6.5 %slice-start.5 = ((s8[6291456]{0:T(1024)(128)(4,1)}), s8[4194304]{0:T(1024)(128)(4,1)S(1)}, s32[]{:S(2)}) async-start(s8[6291456]{0:T(1024)(128)(4,1)} %bitcast.16), calls=%async_computation.5 | async-start | bytes 8388608
  442.5 9.7 %slice-start.2 = ((s8[6291456]{0:T(1024)(128)(4,1)}), s8[4194304]{0:T(1024)(128)(4,1)S(1)}, s32[]{:S(2)}) async-start(s8[6291456]{0:T(1024)(128)(4,1)} %bitcast.14), calls=%async_computation.2 | async-start | bytes 8388608
  448.9 3.2 slice-start.3
  448.9 7.1 %slice-start = ((s8[6291456]{0:T(1024)(128)(4,1)}), s8[4194304]{0:T(1024)(128)(4,1)S(1)}, s32[]{:S(2)}) async-start(s8[6291456]{0:T(1024)(128)(4,1)} %bitcast.12), calls=%async_computation | async-start | bytes 8388608
  452.2 4.8 %slice-start.1 = ((s8[6291456]{0:T(1024)(128)(4,1)}), s8[2097152]{0:T(1024)(128)(4,1)S(1)}, s32[]{:S(2)}) async-start(s8[6291456]{0:T(1024)(128)(4,1)} %bitcast.12), calls=%async_computation.1 | async-start | bytes 4194304
  452.2 8.0 %slice-start.8 = ((s8[6291456]{0:T(1024)(128)(4,1)}), s8[2097152]{0:T(1024)(128)(4,1)S(1)}, s32[]{:S(2)}) async-start(s8[6291456]{0:T(1024)(128)(4,1)} %bitcast.20), calls=%async_computation.8 | async-start | bytes 4194304
  456.9 4.6 slice-start.9
  457.0 7.8 %slice-start.6 = ((s8[6291456]{0:T(1024)(128)(4,1)}), s8[2097152]{0:T(1024)(128)(4,1)S(1)}, s32[]{:S(2)}) async-start(s8[6291456]{0:T(1024)(128)(4,1)} %bitcast.18), calls=%async_computation.6 | async-start | bytes 4194304
  461.6 4.6 slice-start.7

commit v2 on v1

--- a/solution.py
+++ b/solution.py
@@ -10,6 +10,7 @@
 MESH = pl.DeviceIdType.MESH
 CORES = 2
 SIDES = 2
+CUTS = 4
 RELAY = 6
 
 
@@ -147,14 +148,15 @@
         for side in range(SIDES):
             owner = zone * SIDES + side
             unaligned = jnp.logical_not(aligned)
-            send(
-                unaligned,
-                cols(sources[m], 0, main, side),
-                passing.at[m, side],
-                s_cross.at[m, side],
-                r_cross.at[m, side],
-                here(peer),
-            )
+            for k in range(RELAY - 1):
+                send(
+                    unaligned,
+                    cols(sources[m], k * part, part, side),
+                    passing.at[m, side, k],
+                    s_cross.at[m, side, k],
+                    r_cross.at[m, side, k],
+                    here(peer),
+                )
             send(
                 unaligned,
                 cols(sources[m], part, main, side),
@@ -224,17 +226,19 @@
     far_zone = (1 - x) * CORES + c
     for m in range(2):
         for side in range(SIDES):
-            pl.when(aligned)(
-                functools.partial(landed, passing.at[m, side], r_cross.at[m, side])
-            )
-            send(
-                aligned,
-                passing.at[m, side],
-                at(targets[m], fs, 0, main),
-                s_pass.at[m, side],
-                r_main.at[m, fs],
-                (far_zone * SIDES + side, tp),
-            )
+            for k in range(RELAY - 1):
+                held = passing.at[m, side, k]
+                pl.when(aligned)(
+                    functools.partial(landed, held, r_cross.at[m, side, k])
+                )
+                send(
+                    aligned,
+                    held,
+                    at(targets[m], fs, k * part, part),
+                    s_pass.at[m, side, k],
+                    r_main.at[m, fs],
+                    (far_zone * SIDES + side, tp),
+                )
 
     for m in range(2):
         for step in range(2 * SIDES):
@@ -343,7 +347,7 @@
     rows, columns = gate.shape
     fs, tp = lax.axis_size("fs"), lax.axis_size("tp")
     width = columns * tp // fs
-    main = rows - rows // RELAY
+    part = rows // RELAY
     grid_like = jax.ShapeDtypeStruct((rows * fs, width), jnp.bfloat16)
     any_place = pl.BlockSpec(memory_space=pl.ANY)
     dma = pltpu.SemaphoreType.DMA
@@ -357,13 +361,13 @@
         in_specs=[any_place] * 3,
         out_specs=(any_place,) * 3,
         scratch_shapes=[
-            pltpu.VMEM((2, SIDES, main, width), jnp.bfloat16),
+            pltpu.VMEM((2, SIDES, RELAY - 1, part, width), jnp.bfloat16),
             pltpu.VMEM((2, rows, width), jnp.bfloat16),
             pltpu.VMEM(down.shape, jnp.bfloat16),
             dma((2, SIDES)),
-            dma((2, SIDES)),
-            dma((2, SIDES)),
-            dma((2, SIDES)),
+            dma((2, SIDES, RELAY - 1)),
+            dma((2, SIDES, RELAY - 1)),
+            dma((2, SIDES, RELAY - 1)),
             dma((2, fs)),
             dma((2, fs)),
             dma((2, fs)),
@@ -376,6 +380,111 @@
         ],
         compiler_params=pltpu.CompilerParams(has_side_effects=True),
     )(gate, up, down)
+
+
+def half_kernel(
+    normed,
+    gate,
+    up,
+    down,
+    serve_gate,
+    serve_up,
+    serve_down,
+    partial_value,
+    v_gate,
+    v_up,
+    v_down,
+    gate_sum,
+    up_sum,
+    arrive,
+    leave,
+):
+    deep = gate.shape[0] // CUTS
+    wide = down.shape[1] // CUTS
+
+    def rows_of(ref, k):
+        return ref.at[pl.ds(k * deep, deep), :]
+
+    def lanes_of(ref, k):
+        return ref.at[:, pl.ds(k * wide, wide)]
+
+    plan = [(gate, v_gate, serve_gate, rows_of), (up, v_up, serve_up, rows_of)]
+    plan.append((down, v_down, serve_down, lanes_of))
+
+    def coming(m, k):
+        src, held, _, cut = plan[m]
+        return pltpu.make_async_copy(cut(src, k), cut(held, k), arrive.at[m, k])
+
+    def going(m, k):
+        _, held, dst, cut = plan[m]
+        return pltpu.make_async_copy(cut(held, k), cut(dst, k), leave.at[m, k])
+
+    for k in range(CUTS):
+        coming(0, k).start()
+        coming(1, k).start()
+    for k in range(CUTS):
+        coming(2, k).start()
+    for k in range(CUTS):
+        n = normed[:, k * deep : (k + 1) * deep]
+        for m, total in ((0, gate_sum), (1, up_sum)):
+            coming(m, k).wait()
+            going(m, k).start()
+            term = jnp.dot(
+                n,
+                plan[m][1][k * deep : (k + 1) * deep, :],
+                preferred_element_type=jnp.float32,
+            )
+            if k:
+                total[...] += term
+            else:
+                total[...] = term
+    hidden = (jax.nn.silu(gate_sum[...]) * up_sum[...]).astype(jnp.bfloat16)
+    for k in range(CUTS):
+        coming(2, k).wait()
+        going(2, k).start()
+        partial_value[:, k * wide : (k + 1) * wide] = jnp.dot(
+            hidden,
+            v_down[:, k * wide : (k + 1) * wide],
+            preferred_element_type=jnp.float32,
+        ).astype(jnp.bfloat16)
+    for m in range(3):
+        for k in range(CUTS):
+            going(m, k).wait()
+
+
+def half_block(normed, gate, up, down):
+    rows, width = normed.shape
+    vmem = pl.BlockSpec(memory_space=pltpu.VMEM)
+    any_place = pl.BlockSpec(memory_space=pl.ANY)
+    same = lambda a: jax.ShapeDtypeStruct(a.shape, a.dtype)
+    *served, partial_value = pl.pallas_call(
+        half_kernel,
+        out_shape=(same(gate), same(up), same(down), same(normed)),
+        in_specs=[vmem] + [any_place] * 3,
+        out_specs=(any_place,) * 3 + (vmem,),
+        scratch_shapes=[
+            pltpu.VMEM(gate.shape, gate.dtype),
+            pltpu.VMEM(up.shape, up.dtype),
+            pltpu.VMEM(down.shape, down.dtype),
+            pltpu.VMEM((rows, gate.shape[1]), jnp.float32),
+            pltpu.VMEM((rows, gate.shape[1]), jnp.float32),
+            pltpu.SemaphoreType.DMA((3, CUTS)),
+            pltpu.SemaphoreType.DMA((3, CUTS)),
+        ],
+        compiler_params=pltpu.CompilerParams(vmem_limit_bytes=60 * 2**20),
+        cost_estimate=pl.CostEstimate(
+            flops=6 * rows * gate.size, bytes_accessed=12 * gate.size, transcendentals=0
+        ),
+    )(normed, gate, up, down)
+    return served, partial_value
+
+
+def half_block_plain(normed, w_gate, w_rising, w_down):
+    gate_part = jnp.dot(normed, w_gate, preferred_element_type=jnp.float32)
+    rising = jnp.dot(normed, w_rising, preferred_element_type=jnp.float32)
+    hidden = (jax.nn.silu(gate_part) * rising).astype(jnp.bfloat16)
+    partial_value = jnp.dot(hidden, w_down, preferred_element_type=jnp.float32)
+    return (w_gate, w_rising, w_down), partial_value
 
 
 def close_kernel(
@@ -479,18 +588,12 @@
     row_count = gate_first.shape[0]
     offset = lax.axis_index("fs") * row_count
     bring = collect if use_kernels else collect_plain
+    work = half_block if use_kernels else half_block_plain
     finish = close if use_kernels else close_plain
 
     def fold_gain(weight, scales):
         picked = lax.dynamic_slice_in_dim(scales, offset, row_count, 0)
         return (picked[:, None] * weight).astype(jnp.bfloat16)
-
-    def half_step(normed, scales, w_gate, w_rising, w_down):
-        gate_part = jnp.dot(normed, w_gate, preferred_element_type=jnp.float32)
-        rising = jnp.dot(normed, w_rising, preferred_element_type=jnp.float32)
-        hidden = (jax.nn.silu(gate_part) * rising).astype(jnp.bfloat16)
-        partial_value = jnp.dot(hidden, w_down, preferred_element_type=jnp.float32)
-        return finish(partial_value, normed, scales)
 
     first = bring(
         fold_gain(gate_first, gain_first),
@@ -503,8 +606,10 @@
         down_second.astype(jnp.bfloat16),
     )
     normed_zero = plain_norm(tokens).astype(jnp.bfloat16)
-    normed_one = half_step(normed_zero, gain_first, *first)
-    result_rows = half_step(normed_one, gain_second, *second)
+    first, partial_value = work(normed_zero, *first)
+    normed_one = finish(partial_value, normed_zero, gain_first)
+    second, partial_value = work(normed_one, *second)
+    result_rows = finish(partial_value, normed_one, gain_second)
     return (result_rows, *first, *second)
 
 

time: 472 us -> 433 us (0.917)
  matrix products: 24 us -> 0 us
  local copies, waits for them, and re-layouts: 30.2 us -> 6.58 us
  Pallas kernels: 399 us -> 409 us
    pallas_call x0 -> x2, Pallas kernels: none -> 31 us  [half_block(): pl.pallas_call(half_kernel, out_shape=(same(gate), same(up), same(down),...]
    dot_general x4 -> x0, matrix products: 24 us -> none  [the longest x2 15.7 us: half_step(): partial_value = jnp.dot(hidden, w_down, preferred_element_type=jnp.float32)]
    unnamed x37 -> x13, local copies, waits for them, and re-layouts: 28.6 us -> 5.03 us
    pallas_call x2, Pallas kernels: 123 us -> 101 us  [close(): pl.pallas_call(close_kernel, out_shape=jax.ShapeDtypeStruct((rows, width)...]
    convert_element_type x2, other arithmetic: 11.3 us -> 5.34 us  [fold_gain(): return (picked[:, None] * weight).astype(jnp.bfloat16)]
where the time goes in v2:
time: 433 us; the launch traced here: 430 us
  Pallas kernels  409 us (94%)
  other arithmetic  13.8 us (3%)
  local copies, waits for them, and re-layouts  6.58 us (2%)
    pallas_call x2, Pallas kernels, collect(): pl.pallas_call(collect_kernel, out_shape=(grid_like, grid_like, jax.Shape...  277 us
    pallas_call x2, Pallas kernels, close(): pl.pallas_call(close_kernel, out_shape=jax.ShapeDtypeStruct((rows, width)...  101 us
    pallas_call x2, Pallas kernels, half_block(): pl.pallas_call(half_kernel, out_shape=(same(gate), same(up), same(down),...  31 us

profile of v2, /device:TPU:0, one launch (start us, length us, event | category | flops | bytes accessed | tf_op | source)
XLA Modules:
  0.0 429.7 jit_solution(2089913457661362175)
XLA Ops:
  0.6 0.0 copy-start.4
  0.6 1.6 convert_reduce_fusion
  2.2 1.6 fusion.2
  3.8 0.8 dynamic_slice.8
  4.6 0.8 dynamic_slice.9
  5.4 0.0 copy-start.5
  5.4 2.7 fusion.3.normed
  8.1 0.0 copy-done.4
  8.1 0.0 copy-start.1
  8.1 1.3 convert_element_type.28.down
  9.4 0.0 copy-done.5
  9.4 0.0 copy-start
  9.4 1.4 convert_element_type.31.down
  10.7 0.0 copy-done.1
  10.7 1.5 copy-done
  12.2 0.0 copy-start.2
  12.2 0.0 copy-start.3
  12.2 2.7 multiply_convert_fusion
  14.9 0.0 copy-done.2
  14.9 1.3 copy-done.3
  16.2 2.7 multiply_convert_fusion.2
  18.9 137.1 %shard_map.144 = (bf16[3072,1024]{1,0:T(8,128)(2,1)}, bf16[3072,1024]{1,0:T(8,128)(2,1)}, bf16[1024,3072]{1,0:T(8,128)(2,1)}) custom-call(bf16[384,2048]{1,0:T(8,128)(2,1)} %get-tuple-element.38.gate, bf16[384,2048]{1,0:T(8,128)(2,1)} %get-tuple-element.37.up, bf16[1024,768]{1,0:T(8,128)(2,1)} %convert_element_type.28.down), custom_call_target="tpu_custom_call" | custom-call | tf_op jit(solution)/shard_map/pallas_call | solution.py:354
  156.0 15.5 %shard_map.145 = (bf16[3072,1024]{1,0:T(8,128)(2,1)}, bf16[3072,1024]{1,0:T(8,128)(2,1)}, bf16[1024,3072]{1,0:T(8,128)(2,1)}, bf16[160,3072]{1,0:T(8,128)(2,1)}) custom-call(bf16[160,3072]{1,0:T(8,128)(2,1)} %fusion.3.normed, bf16[3072,1024]{1,0:T(8,128)(2,1)} %get-tuple-element.21.gate, bf16[3072,1024]{1,0:T(8,128)(2,1)} %get-tuple-element.22.up, ...), custom_call_target="tpu_custom_call" | custom-call | flops 3019898880 | bytes 37748736 | tf_op jit(solution)/shard_map/pallas_call | solution.py:460
  171.5 50.4 %shard_map.146.normed = bf16[160,3072]{1,0:T(8,128)(2,1)} custom-call(bf16[160,3072]{1,0:T(8,128)(2,1)} %get-tuple-element.24.partial_value, bf16[160,3072]{1,0:T(8,128)(2,1)} %fusion.3.normed, f32[1,3072]{1,0:T(1,128)} %bitcast.2), custom_call_target="tpu_custom_call" | custom-call | tf_op jit(solution)/shard_map/pallas_call | solution.py:558
  221.9 139.7 %shard_map.147 = (bf16[3072,1024]{1,0:T(8,128)(2,1)}, bf16[3072,1024]{1,0:T(8,128)(2,1)}, bf16[1024,3072]{1,0:T(8,128)(2,1)}) custom-call(bf16[384,2048]{1,0:T(8,128)(2,1)} %get-tuple-element.36.gate, bf16[384,2048]{1,0:T(8,128)(2,1)} %get-tuple-element.35.up, bf16[1024,768]{1,0:T(8,128)(2,1)} %convert_element_type.31.down), custom_call_target="tpu_custom_call" | custom-call | tf_op jit(solution)/shard_map/pallas_call | solution.py:354
  361.5 15.5 %shard_map.148 = (bf16[3072,1024]{1,0:T(8,128)(2,1)}, bf16[3072,1024]{1,0:T(8,128)(2,1)}, bf16[1024,3072]{1,0:T(8,128)(2,1)}, bf16[160,3072]{1,0:T(8,128)(2,1)}) custom-call(bf16[160,3072]{1,0:T(8,128)(2,1)} %shard_map.146.normed, bf16[3072,1024]{1,0:T(8,128)(2,1)} %get-tuple-element.25.gate, bf16[3072,1024]{1,0:T(8,128)(2,1)} %get-tuple-element.26.up, ...), custom_call_target="tpu_custom_call" | custom-call | flops 3019898880 | bytes 37748736 | tf_op jit(solution)/shard_map/pallas_call | solution.py:460
  377.0 50.4 %shard_map.149 = bf16[160,3072]{1,0:T(8,128)(2,1)} custom-call(bf16[160,3072]{1,0:T(8,128)(2,1)} %get-tuple-element.28.partial_value, bf16[160,3072]{1,0:T(8,128)(2,1)} %shard_map.146.normed, f32[1,3072]{1,0:T(1,128)} %bitcast.3), custom_call_target="tpu_custom_call" | custom-call | tf_op jit(solution)/shard_map/pallas_call | solution.py:558
  427.5 2.2 copy.17
  (2 shorter events, 0.0 us)
Async XLA Ops:
  0.6 7.4 %copy-start.4 = (f32[1024,768]{1,0:T(8,128)S(1)}, f32[1024,768]{1,0:T(8,128)}, u32[]{:S(2)}) copy-start(f32[1024,768]{1,0:T(8,128)} %param.14) | copy-start | bytes 9437188
  5.4 4.0 copy-start.5
  8.1 2.7 copy-start.1
  9.4 2.9 copy-start
  12.2 2.7 copy-start.2
  12.2 4.0 copy-start.3

commit v3 on v0

v3 whole, which is shorter than its diff:
```python
import functools

import jax
import jax.numpy as jnp
from jax import lax
from jax.experimental import pallas as pl
from jax.experimental.pallas import tpu as pltpu
from jax.sharding import PartitionSpec as P

MESH = pl.DeviceIdType.MESH
CORES = 2
SIDES = 2
CUTS = 4
RELAY = 6


def plain_norm(values):
    values = values.astype(jnp.float32)
    center = jnp.mean(values, axis=-1, keepdims=True)
    spread = jnp.mean(jnp.square(values - center), axis=-1, keepdims=True)
    return (values - center) * lax.rsqrt(spread + 1e-05)


def sum_over_hidden(partial_value):
    pieces = lax.all_to_all(
        partial_value.astype(jnp.bfloat16), "fs", split_axis=1, concat_axis=0, tiled=True
    )
    rows = partial_value.shape[0]
    pieces = pieces.reshape(-1, rows, pieces.shape[1]).astype(jnp.float32)
    summed = jnp.sum(pieces, axis=0).astype(jnp.bfloat16)
    return lax.all_gather(summed, "fs", axis=1, tiled=True).astype(jnp.float32)


def regroup(folded):
    spread = lax.all_to_all(folded, "tp", split_axis=0, concat_axis=1, tiled=True)
    parts = lax.axis_size("fs")
    rows = spread.shape[0]
    owned = lax.all_to_all(spread, "fs", split_axis=1, concat_axis=0, tiled=True)
    owned = owned.reshape(parts, rows, owned.shape[1])
    whole = lax.all_gather(owned, "tp", axis=1, tiled=True)
    return whole.reshape(-1, whole.shape[2])


def collect_plain(gate, up, down):
    return (
        regroup(gate),
        regroup(up),
        lax.all_gather(down, "tp", axis=1, tiled=True),
    )


def half_step_plain(normed, scales, w_gate, w_rising, w_down):
    gate_part = jnp.dot(normed, w_gate, preferred_element_type=jnp.float32)
    rising = jnp.dot(normed, w_rising, preferred_element_type=jnp.float32)
    hidden = (jax.nn.silu(gate_part) * rising).astype(jnp.bfloat16)
    partial_value = jnp.dot(hidden, w_down, preferred_element_type=jnp.float32)
    block = sum_over_hidden(partial_value)
    mixed = 1.6817928 * scales[None, :] * normed.astype(jnp.float32) + 0.5 * block
    return plain_norm(mixed).astype(jnp.bfloat16)


class Send:
    def __init__(self, when, src, dst, send, recv, to):
        self.when = when
        self.copy = pltpu.make_async_remote_copy(
            src_ref=src,
            dst_ref=dst,
            send_sem=send,
            recv_sem=recv,
            device_id=to,
            device_id_type=MESH,
        )

    def start(self):
        if self.when is None:
            self.copy.start()
        else:
            pl.when(self.when)(self.copy.start)

    def wait_send(self):
        if self.when is None:
            self.copy.wait_send()
        else:
            pl.when(self.when)(self.copy.wait_send)


def landed(ref, sem):
    pltpu.make_async_copy(ref, ref, sem).wait()


class Hand:
    def __init__(self, place, send, sources, wholes, down, whole_down, scratch, sems):
        self.__dict__.update(place)
        self.send = send
        self.sources, self.wholes = sources, wholes
        self.down, self.whole_down = down, whole_down
        self.passing, self.bounce, self.bounce_down = scratch
        (
            self.s_plane,
            self.s_cross,
            self.r_cross,
            self.s_pass,
            self.r_main,
            self.r_minor,
            self.s_main,
            self.s_minor,
            self.s_over,
            self.s_down,
            self.r_down,
            self.l_own,
            self.l_down,
        ) = sems
        self.rows = sources[0].shape[0]
        self.width = wholes[0].shape[1]
        self.part = self.rows // RELAY
        self.main = self.rows - self.part
        self.main_at = jnp.where(self.aligned, self.part, 0)
        self.over_at = jnp.where(self.aligned, self.main, 0)
        self.minor_at = jnp.where(self.aligned, 0, self.main)

    def here(self, col):
        return (self.fs, col)

    def cols(self, m, start, size, side):
        return self.sources[m].at[pl.ds(start, size), pl.ds(side * self.width, self.width)]

    def at(self, m, owner, start, size):
        first = pl.multiple_of(owner * self.rows + start, 16)
        return self.wholes[m].at[pl.ds(first, size), :]

    def column(self, col):
        lanes = self.down.shape[1]
        return self.whole_down.at[:, pl.ds(pl.multiple_of(col * lanes, 128), lanes)]

    def own(self, m):
        first = pl.multiple_of(self.y * self.width, 128)
        return self.sources[m].at[:, pl.ds(first, self.width)]

    def cross(self, m, side):
        for k in range(RELAY - 1):
            self.send(
                jnp.logical_not(self.aligned),
                self.cols(m, k * self.part, self.part, side),
                self.passing.at[m, side, k],
                self.s_cross.at[m, side, k],
                self.r_cross.at[m, side, k],
                self.here(self.peer),
            )

    def plane_far(self, m, side):
        self.send(
            jnp.logical_not(self.aligned),
            self.cols(m, self.part, self.main, side),
            self.at(m, self.fs, self.part, self.main),
            self.s_plane.at[m, side],
            self.r_main.at[m, self.fs],
            (self.tp * SIDES + side, self.tp),
        )

    def plane_near(self, m, side):
        owner = self.tp * SIDES + side
        self.send(
            jnp.logical_and(self.aligned, owner != self.fs),
            self.cols(m, 0, self.rows, side),
            self.at(m, self.fs, 0, self.rows),
            self.s_plane.at[m, side],
            self.r_main.at[m, self.fs],
            (owner, self.tp),
        )

    def send_down(self, when):
        for k, to in enumerate((self.peer, self.sibling)):
            self.send(
                when,
                self.down,
                self.column(self.tp),
                self.s_down.at[k],
                self.r_down.at[k],
                self.here(to),
            )

    def home_block(self):
        home = jnp.logical_and(self.aligned, self.primary)
        for m in range(2):
            for sem, to in ((self.s_over, self.peer), (self.s_main, self.sibling)):
                self.send(
                    home,
                    self.own(m),
                    self.at(m, self.fs, 0, self.rows),
                    sem.at[m, self.fs],
                    self.r_main.at[m, self.fs],
                    self.here(to),
                )

    def fetches(self):
        yield None, pltpu.make_async_copy(self.down, self.bounce_down, self.l_down)
        for m in range(2):
            yield jnp.logical_and(self.aligned, self.primary), pltpu.make_async_copy(
                self.own(m), self.bounce.at[m], self.l_own.at[m]
            )

    def puts(self):
        yield None, pltpu.make_async_copy(
            self.bounce_down, self.column(self.tp), self.l_down
        )
        for m in range(2):
            yield jnp.logical_and(self.aligned, self.primary), pltpu.make_async_copy(
                self.bounce.at[m], self.at(m, self.fs, 0, self.rows), self.l_own.at[m]
            )

    def keep(self):
        for when, copy in self.fetches():
            guarded(when, copy.start)
        for when, copy in self.fetches():
            guarded(when, copy.wait)
        for when, copy in self.puts():
            guarded(when, copy.start)

    def kept(self):
        for when, copy in self.puts():
            guarded(when, copy.wait)

    def relay(self, m, side):
        zone = (1 - self.x) * CORES + self.c
        for k in range(RELAY - 1):
            held = self.passing.at[m, side, k]
            guarded(self.aligned, landed, held, self.r_cross.at[m, side, k])
            self.send(
                self.aligned,
                held,
                self.at(m, self.fs, k * self.part, self.part),
                self.s_pass.at[m, side, k],
                self.r_main.at[m, self.fs],
                (zone * SIDES + side, self.tp),
            )

    def near(self, step):
        return self.half * 2 * SIDES + (self.fs + step) % (2 * SIDES)

    def far(self, step):
        return (1 - self.half) * 2 * SIDES + (self.fs + step) % (2 * SIDES)

    def whole_block(self, m, step):
        owner = self.near(step)
        block = self.at(m, owner, 0, self.rows)
        got = self.primary
        if step == 0:
            got = jnp.logical_and(got, jnp.logical_not(self.aligned))
        guarded(got, landed, block, self.r_main.at[m, owner])
        if step:
            self.send(
                jnp.logical_and(self.primary, self.aligned),
                block,
                block,
                self.s_over.at[m, owner],
                self.r_main.at[m, owner],
                self.here(self.peer),
            )
        self.send(
            got,
            block,
            block,
            self.s_main.at[m, owner],
            self.r_main.at[m, owner],
            self.here(self.sibling),
        )

    def pass_down(self):
        got = self.column(self.peer)
        landed(got, self.r_down.at[0])
        self.send(
            None, got, got, self.s_down.at[2], self.r_down.at[2], self.here(self.sibling)
        )

    def main_block(self, m, step):
        owner = self.far(step)
        block = self.at(m, owner, self.main_at, self.main)
        over = self.at(m, owner, self.over_at, self.part)
        guarded(self.primary, landed, block, self.r_main.at[m, owner])
        self.send(
            self.primary,
            over,
            over,
            self.s_over.at[m, owner],
            self.r_minor.at[m, owner],
            self.here(self.peer),
        )
        self.send(
            self.primary,
            block,
            block,
            self.s_main.at[m, owner],
            self.r_main.at[m, owner],
            self.here(self.sibling),
        )

    def minor_block(self, m, step):
        owner = self.far(step)
        block = self.at(m, owner, self.minor_at, self.part)
        guarded(self.primary, landed, block, self.r_minor.at[m, owner])
        self.send(
            self.primary,
            block,
            block,
            self.s_minor.at[m, owner],
            self.r_minor.at[m, owner],
            self.here(self.sibling),
        )

    def second(self):
        other = jnp.logical_not(self.primary)
        for m in range(2):
            for step in range(2 * SIDES):
                owner = self.near(step)
                block = self.at(m, owner, 0, self.rows)
                guarded(other, landed, block, self.r_main.at[m, owner])
                owner = self.far(step)
                block = self.at(m, owner, self.main_at, self.main)
                guarded(other, landed, block, self.r_main.at[m, owner])
                block = self.at(m, owner, self.minor_at, self.part)
                guarded(other, landed, block, self.r_minor.at[m, owner])
        landed(self.column(self.sibling), self.r_down.at[1])
        landed(self.column((1 - self.x) * CORES + 1 - self.c), self.r_down.at[2])


def guarded(when, act, *args):
    if when is None:
        act(*args)
    else:
        pl.when(when)(functools.partial(act, *args))


class Close:
    def __init__(self, place, send, partial_value, landing, summed, full, sems):
        self.__dict__.update(place)
        self.send = send
        self.partial_value, self.landing = partial_value, landing
        self.summed, self.full = summed, full
        self.s_part, self.r_part, self.s_sum, self.r_sum = sems
        self.count = full.shape[0]

    def lanes(self, index):
        width = self.summed.shape[1]
        return pl.ds(pl.multiple_of(index * width, 128), width)

    def scatter(self):
        for step in range(1, self.count):
            to = (self.fs + step) % self.count
            self.send(
                None,
                self.partial_value.at[:, self.lanes(to)],
                self.landing.at[step - 1],
                self.s_part.at[step - 1],
                self.r_part.at[step - 1],
                (to, self.tp),
            )

    def spread(self):
        for step in range(1, self.count):
            landed(self.landing.at[step - 1], self.r_part.at[step - 1])
        total = self.partial_value[:, self.lanes(self.fs)].astype(jnp.float32)
        for step in range(1, self.count):
            total += self.landing[step - 1].astype(jnp.float32)
        self.summed[...] = total.astype(jnp.bfloat16)
        for step in range(1, self.count):
            to = (self.fs + step) % self.count
            self.send(
                None,
                self.summed,
                self.full.at[self.fs],
                self.s_sum.at[step - 1],
                self.r_sum.at[step - 1],
                (to, self.tp),
            )
        self.full[self.fs] = self.summed[...]

    def norm(self, normed, scales, out):
        for step in range(1, self.count):
            came = (self.fs + self.count - step) % self.count
            landed(self.full.at[came], self.r_sum.at[step - 1])
        tall = 16

        def some_rows(index, carry):
            some = pl.ds(pl.multiple_of(index * tall, tall), tall)
            block = jnp.concatenate(
                [self.full[k, some, :].astype(jnp.float32) for k in range(self.count)],
                axis=1,
            )
            mixed = 1.6817928 * scales[...] * normed[some, :].astype(jnp.float32)
            out[some, :] = plain_norm(mixed + 0.5 * block).astype(jnp.bfloat16)
            return carry

        lax.fori_loop(0, out.shape[0] // tall, some_rows, 0)


def placing():
    fs = lax.axis_index("fs")
    tp = lax.axis_index("tp")
    z, x, c = fs // SIDES, tp // CORES, tp % CORES
    return dict(
        fs=fs,
        tp=tp,
        y=fs % SIDES,
        x=x,
        c=c,
        half=z // 2,
        aligned=x == z // 2,
        primary=c == z % 2,
        peer=(1 - x) * CORES + c,
        sibling=x * CORES + 1 - c,
    )


def sender():
    started = []

    def send(*args):
        one = Send(*args)
        one.start()
        started.append(one)

    return send, started


def multiply(normed, plan, sums, partial_value, arrive, leave):
    deep = plan[0][0].shape[0] // CUTS
    wide = plan[2][0].shape[1] // CUTS

    def cut(m, ref, k):
        if m < 2:
            return ref.at[pl.ds(k * deep, deep), :]
        return ref.at[:, pl.ds(k * wide, wide)]

    def coming(m, k):
        src, held, _ = plan[m]
        return pltpu.make_async_copy(cut(m, src, k), cut(m, held, k), arrive.at[m, k])

    def going(m, k):
        _, held, dst = plan[m]
        return pltpu.make_async_copy(cut(m, held, k), cut(m, dst, k), leave.at[m, k])

    def arrived(m, k):
        coming(m, k).wait()
        if plan[m][2] is not None:
            going(m, k).start()

    for k in range(CUTS):
        coming(0, k).start()
        coming(1, k).start()
    for k in range(CUTS):
        coming(2, k).start()
    for k in range(CUTS):
        n = normed[:, k * deep : (k + 1) * deep]
        for m, total in enumerate(sums):
            arrived(m, k)
            term = jnp.dot(
                n,
                plan[m][1][k * deep : (k + 1) * deep, :],
                preferred_element_type=jnp.float32,
            )
            if k:
                total[...] += term
            else:
                total[...] = term
    hidden = (jax.nn.silu(sums[0][...]) * sums[1][...]).astype(jnp.bfloat16)
    for k in range(CUTS):
        arrived(2, k)
        partial_value[:, k * wide : (k + 1) * wide] = jnp.dot(
            hidden,
            plan[2][1][:, k * wide : (k + 1) * wide],
            preferred_element_type=jnp.float32,
        ).astype(jnp.bfloat16)
    return [
        going(m, k) for m in range(3) if plan[m][2] is not None for k in range(CUTS)
    ]


def collect_kernel(*refs):
    (g1, u1, d1, g2, u2, d2, normed, scales), refs = refs[:8], refs[8:]
    (w1, v1, x1, w2, v2, x2, out), refs = refs[:7], refs[7:]
    (passing, bounce, bounce_down), refs = refs[:3], refs[3:]
    (hold_gate, hold_up, hold_down, gate_sum, up_sum), refs = refs[:5], refs[5:]
    (partial_value, landing, summed, full), refs = refs[:4], refs[4:]
    sems, refs = refs[:13], refs[13:]
    arrive, close_sems = refs[0], refs[1:]
    place = placing()
    aligned = place["aligned"]
    unaligned = jnp.logical_not(aligned)
    send, started = sender()
    one, two = (
        Hand(
            place,
            send,
            (gate, up),
            (whole_gate, whole_up),
            down,
            whole_down,
            (passing.at[h], bounce.at[h], bounce_down.at[h]),
            [sem.at[h] for sem in sems],
        )
        for h, (gate, up, down, whole_gate, whole_up, whole_down) in enumerate(
            ((g1, u1, d1, w1, v1, x1), (g2, u2, d2, w2, v2, x2))
        )
    )
    close = Close(place, send, partial_value, landing, summed, full, close_sems)
    turns = [(m, side) for m in range(2) for side in range(SIDES)]

    for m, side in turns:
        one.cross(m, side)
        one.plane_far(m, side)
        one.plane_near(m, side)
    one.send_down(None)
    one.home_block()
    two.cross(0, 0)
    two.plane_far(0, 0)
    two.cross(0, 1)
    one.keep()
    one.relay(0, 0)
    one.whole_block(0, 0)
    one.whole_block(0, 1)
    one.relay(0, 1)
    one.whole_block(0, 2)
    one.whole_block(0, 3)
    one.relay(1, 0)
    one.whole_block(1, 0)
    one.whole_block(1, 1)
    one.relay(1, 1)
    one.whole_block(1, 2)
    one.whole_block(1, 3)
    for m, side in turns:
        two.plane_near(m, side)
    two.send_down(aligned)
    two.home_block()
    one.pass_down()
    for step in range(2 * SIDES):
        one.main_block(0, step)
    two.plane_far(0, 1)
    for step in range(2 * SIDES):
        one.main_block(1, step)
    two.relay(0, 0)
    for m in range(2):
        for step in range(2 * SIDES):
            one.minor_block(m, step)
    one.second()
    one.kept()
    two.relay(0, 1)
    two.cross(1, 0)
    multiply(
        normed,
        ((w1, hold_gate, None), (v1, hold_up, None), (x1, hold_down, None)),
        (gate_sum, up_sum),
        partial_value,
        arrive,
        None,
    )
    close.scatter()
    two.plane_far(1, 0)
    two.cross(1, 1)
    two.send_down(unaligned)
    two.keep()
    two.whole_block(0, 0)
    two.whole_block(0, 1)
    two.whole_block(0, 2)
    close.spread()
    two.plane_far(1, 1)
    two.relay(1, 0)
    two.whole_block(0, 3)
    two.whole_block(1, 0)
    two.whole_block(1, 1)
    two.relay(1, 1)
    two.whole_block(1, 2)
    two.whole_block(1, 3)
    two.pass_down()
    close.norm(normed, scales, out)
    for m in range(2):
        for step in range(2 * SIDES):
            two.main_block(m, step)
    for m in range(2):
        for step in range(2 * SIDES):
            two.minor_block(m, step)
    two.second()
    two.kept()
    for copy in started:
        copy.wait_send()


def collect(first, second, normed, scales):
    gate, _, down = first
    rows, columns = gate.shape
    fs, tp = lax.axis_size("fs"), lax.axis_size("tp")
    width = columns * tp // fs
    part = rows // RELAY
    tall, wide = normed.shape
    piece = wide // fs
    whole = jax.ShapeDtypeStruct((rows * fs, width), jnp.bfloat16)
    whole_down = jax.ShapeDtypeStruct((down.shape[0], down.shape[1] * tp), jnp.bfloat16)
    any_place = pl.BlockSpec(memory_space=pl.ANY)
    vmem = pl.BlockSpec(memory_space=pltpu.VMEM)
    dma = pltpu.SemaphoreType.DMA
    held = lambda *shape: pltpu.VMEM(shape, jnp.bfloat16)
    relayed = dma((2, 2, SIDES, RELAY - 1))
    by_owner = dma((2, 2, fs))
    *weights, normed_one = pl.pallas_call(
        collect_kernel,
        out_shape=(whole, whole, whole_down) * 2
        + (jax.ShapeDtypeStruct(normed.shape, normed.dtype),),
        in_specs=[any_place] * 6 + [vmem] * 2,
        out_specs=(any_place,) * 6 + (vmem,),
        scratch_shapes=[
            held(2, 2, SIDES, RELAY - 1, part, width),
            held(2, 2, rows, width),
            held(2, *down.shape),
            held(*whole.shape),
            held(*whole.shape),
            held(*whole_down.shape),
            pltpu.VMEM((tall, width), jnp.float32),
            pltpu.VMEM((tall, width), jnp.float32),
            held(tall, wide),
            held(fs - 1, tall, piece),
            held(tall, piece),
            held(fs, tall, piece),
            dma((2, 2, SIDES)),
            relayed,
            relayed,
            relayed,
            by_owner,
            by_owner,
            by_owner,
            by_owner,
            by_owner,
            dma((2, 3)),
            dma((2, 3)),
            dma((2, 2)),
            dma((2,)),
            dma((3, CUTS)),
            dma((fs - 1,)),
            dma((fs - 1,)),
            dma((fs - 1,)),
            dma((fs - 1,)),
        ],
        compiler_params=pltpu.CompilerParams(
            has_side_effects=True, vmem_limit_bytes=60 * 2**20
        ),
    )(*first, *second, normed, scales[None, :])
    return weights[:3], weights[3:], normed_one


def serve_kernel(*refs):
    normed, refs = refs[0], refs[1:]
    first, second, refs = refs[:3], refs[3:6], refs[6:]
    out_first, out_second, refs = refs[:3], refs[3:6], refs[6:]
    partial_value, refs = refs[0], refs[1:]
    held_first, held_second, refs = refs[:3], refs[3:6], refs[6:]
    gate_sum, up_sum, arrive, leave, through, away = refs
    ins = [
        pltpu.make_async_copy(first[m], held_first[m], through.at[m]) for m in range(3)
    ]
    outs = [
        pltpu.make_async_copy(held_first[m], out_first[m], away.at[m]) for m in range(3)
    ]
    goings = multiply(
        normed,
        list(zip(second, held_second, out_second)),
        (gate_sum, up_sum),
        partial_value,
        arrive,
        leave,
    )
    for copy in ins:
        copy.start()
    for copy, next_copy in zip(ins, outs):
        copy.wait()
        next_copy.start()
    for copy in goings + outs:
        copy.wait()


def serve(normed, first, second):
    rows, width = normed.shape
    gate = first[0]
    vmem = pl.BlockSpec(memory_space=pltpu.VMEM)
    any_place = pl.BlockSpec(memory_space=pl.ANY)
    same = lambda a: jax.ShapeDtypeStruct(a.shape, a.dtype)
    dma = pltpu.SemaphoreType.DMA
    weights = (*first, *second)
    *served, partial_value = pl.pallas_call(
        serve_kernel,
        out_shape=tuple(same(a) for a in weights) + (same(normed),),
        in_specs=[vmem] + [any_place] * 6,
        out_specs=(any_place,) * 6 + (vmem,),
        scratch_shapes=[pltpu.VMEM(a.shape, a.dtype) for a in weights]
        + [
            pltpu.VMEM((rows, gate.shape[1]), jnp.float32),
            pltpu.VMEM((rows, gate.shape[1]), jnp.float32),
            dma((3, CUTS)),
            dma((3, CUTS)),
            dma((3,)),
            dma((3,)),
        ],
        compiler_params=pltpu.CompilerParams(vmem_limit_bytes=60 * 2**20),
        cost_estimate=pl.CostEstimate(
            flops=6 * rows * gate.size, bytes_accessed=24 * gate.size, transcendentals=0
        ),
    )(normed, *weights)
    return served[:3], served[3:], partial_value


def close_kernel(
    partial_value, normed, scales, out, landing, summed, full, *sems
):
    send, started = sender()
    close = Close(placing(), send, partial_value, landing, summed, full, sems)
    close.scatter()
    close.spread()
    close.norm(normed, scales, out)
    for copy in started:
        copy.wait_send()


def close(partial_value, normed, scales):
    rows, width = normed.shape
    count = lax.axis_size("fs")
    piece = width // count
    vmem = pl.BlockSpec(memory_space=pltpu.VMEM)
    dma = pltpu.SemaphoreType.DMA
    return pl.pallas_call(
        close_kernel,
        out_shape=jax.ShapeDtypeStruct((rows, width), jnp.bfloat16),
        in_specs=[vmem] * 3,
        out_specs=vmem,
        scratch_shapes=[
            pltpu.VMEM((count - 1, rows, piece), jnp.bfloat16),
            pltpu.VMEM((rows, piece), jnp.bfloat16),
            pltpu.VMEM((count, rows, piece), jnp.bfloat16),
            dma((count - 1,)),
            dma((count - 1,)),
            dma((count - 1,)),
            dma((count - 1,)),
        ],
        compiler_params=pltpu.CompilerParams(has_side_effects=True),
    )(partial_value, normed, scales[None, :])


def on_device(
    use_kernels,
    tokens,
    gain_first,
    gain_second,
    gate_first,
    up_first,
    down_first,
    gate_second,
    up_second,
    down_second,
):
    row_count = gate_first.shape[0]
    offset = lax.axis_index("fs") * row_count

    def fold_gain(weight, scales):
        picked = lax.dynamic_slice_in_dim(scales, offset, row_count, 0)
        return (picked[:, None] * weight).astype(jnp.bfloat16)

    first = (
        fold_gain(gate_first, gain_first),
        fold_gain(up_first, gain_first),
        down_first.astype(jnp.bfloat16),
    )
    second = (
        fold_gain(gate_second, gain_second),
        fold_gain(up_second, gain_second),
        down_second.astype(jnp.bfloat16),
    )
    normed_zero = plain_norm(tokens).astype(jnp.bfloat16)
    if use_kernels:
        first, second, normed_one = collect(first, second, normed_zero, gain_first)
        first, second, partial_value = serve(normed_one, first, second)
        result_rows = close(partial_value, normed_one, gain_second)
    else:
        first, second = collect_plain(*first), collect_plain(*second)
        normed_one = half_step_plain(normed_zero, gain_first, *first)
        result_rows = half_step_plain(normed_one, gain_second, *second)
    return (result_rows, *first, *second)


def solution(mesh):
    fs, tp = mesh.shape["fs"], mesh.shape["tp"]
    use_kernels = tp == 2 * CORES and fs == tp * SIDES
    placed = (P("tp", None), P(), P()) + (P("fs", "tp"),) * 6
    served = (P(None, "fs"), P(None, "fs"), P("fs", None))
    return jax.shard_map(
        functools.partial(on_device, use_kernels),
        mesh=mesh,
        in_specs=placed,
        out_specs=(P("tp", None),) + served + served,
        check_vma=False,
    )
```

time: 531 us -> 417 us (0.79)
  Pallas kernels: 0 us -> 393 us
  blocking collectives: 365 us -> 0 us
  local copies, waits for them, and re-layouts: 74 us -> 3.77 us
  waiting for transfers between devices: 29.1 us -> 0 us
  matrix products: 16.4 us -> 0 us
  between operations: 14.8 us -> 0.69 us
  starting transfers between devices: 7.57 us -> 0 us
    pallas_call x0 -> x3, Pallas kernels: none -> 393 us  [the longest x1 306 us: collect(): pl.pallas_call(collect_kernel, out_shape=(whole, whole, whole_down) * 2 +...]
    all_to_all x8 -> x0, blocking collectives: 298 us -> none  [the longest x4 172 us: regroup(): lax.all_to_all(spread, 'fs', split_axis=1, concat_axis=0, tiled=True)]
    all_gather x2 -> x0, blocking collectives: 67.3 us -> none  [sum_over_hidden(): return lax.all_gather(summed, 'fs', axis=1, tiled=True).astype(jnp.float32)]
    all_gather x4 -> x0, local copies, waits for them, and re-layouts: 36.9 us -> none  [regroup(): whole = lax.all_gather(owned, 'tp', axis=1, tiled=True)]
    all_to_all x2 -> x0, waiting for transfers between devices: 28.4 us -> none  [sum_over_hidden(): lax.all_to_all(partial_value.astype(jnp.bfloat16), 'fs', split_axis=1, co...]
    all_to_all x18 -> x0, local copies, waits for them, and re-layouts: 25.8 us -> none  [the longest x12 18.8 us: regroup(): lax.all_to_all(spread, 'fs', split_axis=1, concat_axis=0, tiled=True)]
    dot_general x4 -> x0, matrix products: 16.4 us -> none  [the longest x2 13.9 us: half_step(): partial_value = jnp.dot(hidden, w_down, preferred_element_type=jnp.float32)]
    unnamed x20 -> x9, local copies, waits for them, and re-layouts: 10.4 us -> 2.22 us
  transfers between devices with their start and end apart: 8 -> 0, of which waited for: 3 -> 0; matrix products, arithmetic and copies ran while one was open for 14% -> 0% of each run, Pallas kernels for 0% -> 0%
where the time goes in v3:
time: 417 us; the launch traced here: 414 us
  Pallas kernels  393 us (94%)
  other arithmetic  16.5 us (4%)
    pallas_call x1, Pallas kernels, collect(): pl.pallas_call(collect_kernel, out_shape=(whole, whole, whole_down) * 2 +...  306 us
    pallas_call x1, Pallas kernels, close(): pl.pallas_call(close_kernel, out_shape=jax.ShapeDtypeStruct((rows, width)...  58.7 us
    pallas_call x1, Pallas kernels, serve(): pl.pallas_call(serve_kernel, out_shape=tuple((same(a) for a in weights))...  28.6 us

profile of v3, /device:TPU:0, one launch (start us, length us, event | category | flops | bytes accessed | tf_op | source)
XLA Modules:
  0.0 413.8 jit_solution(15830305414605118157)
XLA Ops:
  0.6 0.0 copy-start.3
  0.6 1.6 convert_reduce_fusion
  2.2 1.6 fusion.2
  3.8 0.8 dynamic_slice.8
  4.6 0.8 dynamic_slice.9
  5.4 2.5 fusion.3.refs_6_
  7.9 0.0 copy-start.1
  7.9 0.0 copy-start.2
  7.9 3.3 convert_element_type.26.refs_2_
  11.2 0.0 copy-start
  11.2 3.3 convert_element_type.29.refs_5_
  14.6 0.0 copy-done.3
  14.6 0.0 copy-done.1
  14.6 0.0 copy-done.2
  14.6 0.0 copy-done
  14.6 4.1 multiply_convert_fusion
  18.7 305.7 %shard_map.144 = (bf16[3072,1024]{1,0:T(8,128)(2,1)}, bf16[3072,1024]{1,0:T(8,128)(2,1)}, bf16[1024,3072]{1,0:T(8,128)(2,1)}, bf16[3072,1024]{1,0:T(8,128)(2,1)}...) custom-call(bf16[384,2048]{1,0:T(8,128)(2,1)} %get-tuple-element.39.refs_0_, ...), custom_call_target="tpu_custom_call" | custom-call | tf_op jit(solution)/shard_map/pallas_call | solution.py:603
  324.4 28.6 %shard_map.145 = (bf16[3072,1024]{1,0:T(8,128)(2,1)}, bf16[3072,1024]{1,0:T(8,128)(2,1)}, bf16[1024,3072]{1,0:T(8,128)(2,1)}, bf16[3072,1024]{1,0:T(8,128)(2,1)}...) custom-call(bf16[160,3072]{1,0:T(8,128)(2,1)} %get-tuple-element.21.refs_0_.normed, ...), custom_call_target="tpu_custom_call" | custom-call | flops 3019898880 | bytes 75497472 | tf_op jit(solution)/shard_map/pallas_call | solution.py:686
  352.9 58.7 %shard_map.146 = bf16[160,3072]{1,0:T(8,128)(2,1)} custom-call(bf16[160,3072]{1,0:T(8,128)(2,1)} %get-tuple-element.28.partial_value, bf16[160,3072]{1,0:T(8,128)(2,1)} %get-tuple-element.21.refs_0_.normed, f32[1,3072]{1,0:T(1,128)} %bitcast.2), custom_call_target="tpu_custom_call" | custom-call | tf_op jit(solution)/shard_map/pallas_call | solution.py:726
  411.6 2.2 copy.17
  (2 shorter events, 0.0 us)
Async XLA Ops:
  0.6 13.9 %copy-start.3 = (f32[384,2048]{1,0:T(8,128)S(1)}, f32[384,2048]{1,0:T(8,128)}, u32[]{:S(2)}) copy-start(f32[384,2048]{1,0:T(8,128)} %param.13) | copy-start | bytes 9437188
  7.9 6.7 %copy-start.1 = (f32[384,2048]{1,0:T(8,128)S(1)}, f32[384,2048]{1,0:T(8,128)}, u32[]{:S(2)}) copy-start(f32[384,2048]{1,0:T(8,128)} %param.15) | copy-start | bytes 9437188
  7.9 6.7 %copy-start.2 = (f32[384,2048]{1,0:T(8,128)S(1)}, f32[384,2048]{1,0:T(8,128)}, u32[]{:S(2)}) copy-start(f32[384,2048]{1,0:T(8,128)} %param.12) | copy-start | bytes 9437188
  11.2 3.4 copy-start

commit v4 on v3

--- a/solution.py
+++ b/solution.py
@@ -331,66 +331,140 @@
 
 
 class Close:
-    def __init__(self, place, send, partial_value, landing, summed, full, sems):
+    def __init__(self, place, send, partial_value, beside, halves, along, full, sems):
         self.__dict__.update(place)
         self.send = send
-        self.partial_value, self.landing = partial_value, landing
-        self.summed, self.full = summed, full
-        self.s_part, self.r_part, self.s_sum, self.r_sum = sems
-        self.count = full.shape[0]
-
-    def lanes(self, index):
-        width = self.summed.shape[1]
-        return pl.ds(pl.multiple_of(index * width, 128), width)
+        self.partial_value, self.beside = partial_value, beside
+        self.halves, self.along, self.full = halves, along, full
+        (
+            self.s_y,
+            self.r_y,
+            self.s_z,
+            self.r_z,
+            self.s_up,
+            self.r_up,
+            self.s_side,
+            self.r_side,
+        ) = sems
+        self.zones = beside.shape[0]
+
+    def piece(self, zone, side):
+        width = self.full.shape[2]
+        first = (zone * SIDES + side) * width
+        return pl.ds(pl.multiple_of(first, 128), width)
+
+    def zone(self, step):
+        return (self.z + self.zones + step) % self.zones
+
+    def held(self, zone, side):
+        return self.full.at[zone * SIDES + side]
 
     def scatter(self):
-        for step in range(1, self.count):
-            to = (self.fs + step) % self.count
+        for step in (*range(1, self.zones), 0):
             self.send(
                 None,
-                self.partial_value.at[:, self.lanes(to)],
-                self.landing.at[step - 1],
-                self.s_part.at[step - 1],
-                self.r_part.at[step - 1],
-                (to, self.tp),
-            )
-
-    def spread(self):
-        for step in range(1, self.count):
-            landed(self.landing.at[step - 1], self.r_part.at[step - 1])
-        total = self.partial_value[:, self.lanes(self.fs)].astype(jnp.float32)
-        for step in range(1, self.count):
-            total += self.landing[step - 1].astype(jnp.float32)
-        self.summed[...] = total.astype(jnp.bfloat16)
-        for step in range(1, self.count):
-            to = (self.fs + step) % self.count
+                self.partial_value.at[:, self.piece(self.zone(step), 1 - self.y)],
+                self.beside.at[step],
+                self.s_y.at[step],
+                self.r_y.at[step],
+                (self.z * SIDES + 1 - self.y, self.tp),
+            )
+
+    def both_sides(self, step):
+        landed(self.beside.at[step], self.r_y.at[step])
+        mine = self.partial_value[:, self.piece(self.zone(step), self.y)]
+        return mine.astype(jnp.float32) + self.beside[step].astype(jnp.float32)
+
+    def halve(self):
+        for step in range(1, self.zones):
+            self.halves[step - 1] = self.both_sides(step).astype(jnp.bfloat16)
             self.send(
                 None,
-                self.summed,
-                self.full.at[self.fs],
-                self.s_sum.at[step - 1],
-                self.r_sum.at[step - 1],
-                (to, self.tp),
-            )
-        self.full[self.fs] = self.summed[...]
+                self.halves.at[step - 1],
+                self.along.at[step - 1],
+                self.s_z.at[step - 1],
+                self.r_z.at[step - 1],
+                (self.zone(step) * SIDES + self.y, self.tp),
+            )
+
+    def to_side(self, step, block):
+        self.send(
+            None,
+            block,
+            block,
+            self.s_side.at[step],
+            self.r_side.at[step],
+            (self.z * SIDES + 1 - self.y, self.tp),
+        )
+
+    def spread(self):
+        total = self.both_sides(0)
+        for step in range(1, self.zones):
+            landed(self.along.at[step - 1], self.r_z.at[step - 1])
+            total += self.along[step - 1].astype(jnp.float32)
+        self.full[self.fs] = total.astype(jnp.bfloat16)
+        block = self.held(self.z, self.y)
+        for step in range(1, self.zones):
+            self.send(
+                None,
+                block,
+                block,
+                self.s_up.at[step - 1],
+                self.r_up.at[step - 1],
+                (self.zone(step) * SIDES + self.y, self.tp),
+            )
+        self.to_side(0, block)
+
+    def side(self):
+        for step in range(1, self.zones):
+            block = self.held(self.zone(-step), self.y)
+            landed(block, self.r_up.at[step - 1])
+            self.to_side(step, block)
 
     def norm(self, normed, scales, out):
-        for step in range(1, self.count):
-            came = (self.fs + self.count - step) % self.count
-            landed(self.full.at[came], self.r_sum.at[step - 1])
-        tall = 16
-
-        def some_rows(index, carry):
-            some = pl.ds(pl.multiple_of(index * tall, tall), tall)
+        for step in range(self.zones):
+            landed(self.held(self.zone(-step), 1 - self.y), self.r_side.at[step])
+
+        def mixed(some):
             block = jnp.concatenate(
-                [self.full[k, some, :].astype(jnp.float32) for k in range(self.count)],
+                [
+                    self.full[k, some, :].astype(jnp.float32)
+                    for k in range(self.full.shape[0])
+                ],
                 axis=1,
             )
-            mixed = 1.6817928 * scales[...] * normed[some, :].astype(jnp.float32)
-            out[some, :] = plain_norm(mixed + 0.5 * block).astype(jnp.bfloat16)
-            return carry
-
-        lax.fori_loop(0, out.shape[0] // tall, some_rows, 0)
+            old = 1.6817928 * scales[...] * normed[some, :].astype(jnp.float32)
+            return old + 0.5 * block
+
+        norm_rows(mixed, out)
+
+
+def norm_rows(values, out):
+    tall = 16
+
+    def some_rows(index, carry):
+        some = pl.ds(pl.multiple_of(index * tall, tall), tall)
+        out[some, :] = plain_norm(values(some)).astype(jnp.bfloat16)
+        return carry
+
+    lax.fori_loop(0, out.shape[0] // tall, some_rows, 0)
+
+
+def greet(partners):
+    barrier = pltpu.get_barrier_semaphore()
+    for partner in partners:
+        pl.semaphore_signal(barrier, inc=1, device_id=partner, device_id_type=MESH)
+    pl.semaphore_wait(barrier, len(partners))
+
+
+def close_scratch(rows, width, count):
+    held = lambda many: pltpu.VMEM((many, rows, width // count), jnp.bfloat16)
+    zones = count // SIDES
+    dma = pltpu.SemaphoreType.DMA
+    sems = [dma((many,)) for many in (zones, zones - 1, zones - 1, zones)]
+    return [held(zones), held(zones - 1), held(zones - 1), held(count)] + [
+        sem for sem in sems for _ in range(2)
+    ]
 
 
 def placing():
@@ -400,6 +474,7 @@
     return dict(
         fs=fs,
         tp=tp,
+        z=z,
         y=fs % SIDES,
         x=x,
         c=c,
@@ -422,7 +497,7 @@
     return send, started
 
 
-def multiply(normed, plan, sums, partial_value, arrive, leave):
+def multiply(normed, plan, sums, partial_value, arrive, leave, others=()):
     deep = plan[0][0].shape[0] // CUTS
     wide = plan[2][0].shape[1] // CUTS
 
@@ -449,6 +524,8 @@
         coming(1, k).start()
     for k in range(CUTS):
         coming(2, k).start()
+    for copy in others:
+        copy.start()
     for k in range(CUTS):
         n = normed[:, k * deep : (k + 1) * deep]
         for m, total in enumerate(sums):
@@ -476,14 +553,20 @@
 
 
 def collect_kernel(*refs):
-    (g1, u1, d1, g2, u2, d2, normed, scales), refs = refs[:8], refs[8:]
+    (g1, u1, d1, g2, u2, d2, tokens, scales), refs = refs[:8], refs[8:]
     (w1, v1, x1, w2, v2, x2, out), refs = refs[:7], refs[7:]
     (passing, bounce, bounce_down), refs = refs[:3], refs[3:]
     (hold_gate, hold_up, hold_down, gate_sum, up_sum), refs = refs[:5], refs[5:]
-    (partial_value, landing, summed, full), refs = refs[:4], refs[4:]
+    (normed, partial_value), refs = refs[:2], refs[2:]
     sems, refs = refs[:13], refs[13:]
-    arrive, close_sems = refs[0], refs[1:]
+    arrive, close_scratches = refs[0], refs[1:]
     place = placing()
+    fs, tp = place["fs"], place["tp"]
+    count = lax.axis_size("fs")
+    greet(
+        [((fs + step) % count, tp) for step in range(1, count)]
+        + [(fs, place["peer"]), (fs, place["sibling"])]
+    )
     aligned = place["aligned"]
     unaligned = jnp.logical_not(aligned)
     send, started = sender()
@@ -502,7 +585,7 @@
             ((g1, u1, d1, w1, v1, x1), (g2, u2, d2, w2, v2, x2))
         )
     )
-    close = Close(place, send, partial_value, landing, summed, full, close_sems)
+    close = Close(place, send, partial_value, *close_scratches[:4], close_scratches[4:])
     turns = [(m, side) for m in range(2) for side in range(SIDES)]
 
     for m, side in turns:
@@ -531,6 +614,7 @@
         two.plane_near(m, side)
     two.send_down(aligned)
     two.home_block()
+    norm_rows(lambda some: tokens[some, :], normed)
     one.pass_down()
     for step in range(2 * SIDES):
         one.main_block(0, step)
@@ -554,22 +638,24 @@
         None,
     )
     close.scatter()
-    two.plane_far(1, 0)
     two.cross(1, 1)
     two.send_down(unaligned)
     two.keep()
     two.whole_block(0, 0)
+    close.halve()
+    two.plane_far(1, 0)
+    two.relay(1, 0)
     two.whole_block(0, 1)
     two.whole_block(0, 2)
     close.spread()
     two.plane_far(1, 1)
-    two.relay(1, 0)
+    two.relay(1, 1)
     two.whole_block(0, 3)
     two.whole_block(1, 0)
     two.whole_block(1, 1)
-    two.relay(1, 1)
     two.whole_block(1, 2)
     two.whole_block(1, 3)
+    close.side()
     two.pass_down()
     close.norm(normed, scales, out)
     for m in range(2):
@@ -584,14 +670,13 @@
         copy.wait_send()
 
 
-def collect(first, second, normed, scales):
+def collect(first, second, tokens, scales):
     gate, _, down = first
     rows, columns = gate.shape
     fs, tp = lax.axis_size("fs"), lax.axis_size("tp")
     width = columns * tp // fs
     part = rows // RELAY
-    tall, wide = normed.shape
-    piece = wide // fs
+    tall, wide = tokens.shape
     whole = jax.ShapeDtypeStruct((rows * fs, width), jnp.bfloat16)
     whole_down = jax.ShapeDtypeStruct((down.shape[0], down.shape[1] * tp), jnp.bfloat16)
     any_place = pl.BlockSpec(memory_space=pl.ANY)
@@ -603,7 +688,7 @@
     *weights, normed_one = pl.pallas_call(
         collect_kernel,
         out_shape=(whole, whole, whole_down) * 2
-        + (jax.ShapeDtypeStruct(normed.shape, normed.dtype),),
+        + (jax.ShapeDtypeStruct(tokens.shape, tokens.dtype),),
         in_specs=[any_place] * 6 + [vmem] * 2,
         out_specs=(any_place,) * 6 + (vmem,),
         scratch_shapes=[
@@ -616,9 +701,7 @@
             pltpu.VMEM((tall, width), jnp.float32),
             pltpu.VMEM((tall, width), jnp.float32),
             held(tall, wide),
-            held(fs - 1, tall, piece),
-            held(tall, piece),
-            held(fs, tall, piece),
+            held(tall, wide),
             dma((2, 2, SIDES)),
             relayed,
             relayed,
@@ -633,15 +716,12 @@
             dma((2, 2)),
             dma((2,)),
             dma((3, CUTS)),
-            dma((fs - 1,)),
-            dma((fs - 1,)),
-            dma((fs - 1,)),
-            dma((fs - 1,)),
+            *close_scratch(tall, wide, fs),
         ],
         compiler_params=pltpu.CompilerParams(
-            has_side_effects=True, vmem_limit_bytes=60 * 2**20
+            has_side_effects=True, collective_id=0, vmem_limit_bytes=60 * 2**20
         ),
-    )(*first, *second, normed, scales[None, :])
+    )(*first, *second, tokens, scales[None, :])
     return weights[:3], weights[3:], normed_one
 
 
@@ -665,9 +745,8 @@
         partial_value,
         arrive,
         leave,
-    )
-    for copy in ins:
-        copy.start()
+        ins,
+    )
     for copy, next_copy in zip(ins, outs):
         copy.wait()
         next_copy.start()
@@ -705,13 +784,18 @@
     return served[:3], served[3:], partial_value
 
 
-def close_kernel(
-    partial_value, normed, scales, out, landing, summed, full, *sems
-):
+def close_kernel(partial_value, normed, scales, out, *scratches):
+    place = placing()
     send, started = sender()
-    close = Close(placing(), send, partial_value, landing, summed, full, sems)
+    close = Close(place, send, partial_value, *scratches[:4], scratches[4:])
+    greet(
+        [(close.zone(step) * SIDES + close.y, close.tp) for step in range(1, close.zones)]
+        + [(close.z * SIDES + 1 - close.y, close.tp)]
+    )
     close.scatter()
+    close.halve()
     close.spread()
+    close.side()
     close.norm(normed, scales, out)
     for copy in started:
         copy.wait_send()
@@ -719,25 +803,14 @@
 
 def close(partial_value, normed, scales):
     rows, width = normed.shape
-    count = lax.axis_size("fs")
-    piece = width // count
     vmem = pl.BlockSpec(memory_space=pltpu.VMEM)
-    dma = pltpu.SemaphoreType.DMA
     return pl.pallas_call(
         close_kernel,
         out_shape=jax.ShapeDtypeStruct((rows, width), jnp.bfloat16),
         in_specs=[vmem] * 3,
         out_specs=vmem,
-        scratch_shapes=[
-            pltpu.VMEM((count - 1, rows, piece), jnp.bfloat16),
-            pltpu.VMEM((rows, piece), jnp.bfloat16),
-            pltpu.VMEM((count, rows, piece), jnp.bfloat16),
-            dma((count - 1,)),
-            dma((count - 1,)),
-            dma((count - 1,)),
-            dma((count - 1,)),
-        ],
-        compiler_params=pltpu.CompilerParams(has_side_effects=True),
+        scratch_shapes=close_scratch(rows, width, lax.axis_size("fs")),
+        compiler_params=pltpu.CompilerParams(has_side_effects=True, collective_id=1),
     )(partial_value, normed, scales[None, :])
 
 
@@ -770,13 +843,13 @@
         fold_gain(up_second, gain_second),
         down_second.astype(jnp.bfloat16),
     )
-    normed_zero = plain_norm(tokens).astype(jnp.bfloat16)
     if use_kernels:
-        first, second, normed_one = collect(first, second, normed_zero, gain_first)
+        first, second, normed_one = collect(first, second, tokens, gain_first)
         first, second, partial_value = serve(normed_one, first, second)
         result_rows = close(partial_value, normed_one, gain_second)
     else:
         first, second = collect_plain(*first), collect_plain(*second)
+        normed_zero = plain_norm(tokens).astype(jnp.bfloat16)
         normed_one = half_step_plain(normed_zero, gain_first, *first)
         result_rows = half_step_plain(normed_one, gain_second, *second)
     return (result_rows, *first, *second)

time: 417 us -> 378 us (0.906)
  Pallas kernels: 393 us -> 359 us
    pallas_call x1, Pallas kernels: 58.7 us -> 40.1 us  [close(): pl.pallas_call(close_kernel, out_shape=jax.ShapeDtypeStruct((rows, width)...]
    pallas_call x1, Pallas kernels: 306 us -> 293 us  [collect(): pl.pallas_call(collect_kernel, out_shape=(whole, whole, whole_down) * 2 +...]
where the time goes in v4:
time: 378 us; the launch traced here: 376 us
  Pallas kernels  359 us (95%)
  other arithmetic  12.6 us (3%)
    pallas_call x1, Pallas kernels, collect(): pl.pallas_call(collect_kernel, out_shape=(whole, whole, whole_down) * 2 +...  293 us
    pallas_call x1, Pallas kernels, close(): pl.pallas_call(close_kernel, out_shape=jax.ShapeDtypeStruct((rows, width)...  40.1 us
    pallas_call x1, Pallas kernels, serve(): pl.pallas_call(serve_kernel, out_shape=tuple((same(a) for a in weights))...  25.9 us

profile of v4, /device:TPU:0, one launch (start us, length us, event | category | flops | bytes accessed | tf_op | source)
XLA Modules:
  0.0 376.2 jit_solution(2780528131277202393)
XLA Ops:
  0.6 0.8 dynamic_slice.8
  1.4 0.8 dynamic_slice.9
  2.2 0.0 copy-start.1
  2.2 0.0 copy-start.2
  2.2 3.3 convert_element_type.20.refs_2_
  5.5 0.0 copy-start
  5.5 3.3 convert_element_type.23.refs_5_
  8.9 0.0 copy-done.1
  8.9 0.0 copy-done.2
  8.9 0.0 copy-done
  8.9 5.9 %multiply_convert_fusion = (bf16[384,2048]{1,0:T(8,128)(2,1)}, bf16[384,2048]{1,0:T(8,128)(2,1)}, bf16[384,2048]{1,0:T(8,128)(2,1)}, bf16[384,2048]{1,0:T(8,128)(2,1)}) fusion(f32[384,2048]{1,0:T(8,128)S(1)} %copy-done, f32[384]{0:T(512)S(1)} %dynamic_slice.9, f32[384,2048]{1,0:T(8,128)S(1)} %copy-done.1, f32[384,2048]{1,0:T(8,128)S(1)} %copy-done.2, ...), kind=kLoop, calls=%fused_computation | loop fusion | flops 6291456 | bytes 18877440 | tf_op jit(solution)/shard_map/convert_element_type | solution.py:834
  14.8 293.1 %shard_map.144 = (bf16[3072,1024]{1,0:T(8,128)(2,1)}, bf16[3072,1024]{1,0:T(8,128)(2,1)}, bf16[1024,3072]{1,0:T(8,128)(2,1)}, bf16[3072,1024]{1,0:T(8,128)(2,1)}...) custom-call(bf16[384,2048]{1,0:T(8,128)(2,1)} %get-tuple-element.39.refs_0_, ...), custom_call_target="tpu_custom_call" | custom-call | tf_op jit(solution)/shard_map/pallas_call | solution.py:688
  307.9 25.9 %shard_map.145 = (bf16[3072,1024]{1,0:T(8,128)(2,1)}, bf16[3072,1024]{1,0:T(8,128)(2,1)}, bf16[1024,3072]{1,0:T(8,128)(2,1)}, bf16[3072,1024]{1,0:T(8,128)(2,1)}...) custom-call(bf16[160,3072]{1,0:T(8,128)(2,1)} %get-tuple-element.21.refs_0_.normed, ...), custom_call_target="tpu_custom_call" | custom-call | flops 3019898880 | bytes 75497472 | tf_op jit(solution)/shard_map/pallas_call | solution.py:765
  333.9 40.1 %shard_map.146 = bf16[160,3072]{1,0:T(8,128)(2,1)} custom-call(bf16[160,3072]{1,0:T(8,128)(2,1)} %get-tuple-element.28.partial_value, bf16[160,3072]{1,0:T(8,128)(2,1)} %get-tuple-element.21.refs_0_.normed, f32[1,3072]{1,0:T(1,128)} %bitcast.2), custom_call_target="tpu_custom_call" | custom-call | tf_op jit(solution)/shard_map/pallas_call | solution.py:807
  374.0 2.2 copy.17
Async XLA Ops:
  2.2 6.7 %copy-start.1 = (f32[384,2048]{1,0:T(8,128)S(1)}, f32[384,2048]{1,0:T(8,128)}, u32[]{:S(2)}) copy-start(f32[384,2048]{1,0:T(8,128)} %param.15) | copy-start | bytes 9437188
  2.2 6.7 %copy-start.2 = (f32[384,2048]{1,0:T(8,128)S(1)}, f32[384,2048]{1,0:T(8,128)}, u32[]{:S(2)}) copy-start(f32[384,2048]{1,0:T(8,128)} %param.12) | copy-start | bytes 9437188
  5.5 3.3 copy-start

commit v5 on v4

--- a/solution.py
+++ b/solution.py
@@ -10,8 +10,11 @@
 MESH = pl.DeviceIdType.MESH
 CORES = 2
 SIDES = 2
+COLLECT_VMEM = 20 * 2**20
+SERVE_VMEM = 16 * 2**20
 CUTS = 4
-RELAY = 6
+FAR = 5, 24
+CHUNKS = 4
 
 
 def plain_norm(values):
@@ -88,13 +91,22 @@
     pltpu.make_async_copy(ref, ref, sem).wait()
 
 
+def far_part(rows):
+    return rows * FAR[0] // FAR[1] // 16 * 16
+
+
+def chunks(rows):
+    edges = [rows // 16 * k // CHUNKS * 16 for k in range(CHUNKS + 1)]
+    return [(a, b - a) for a, b in zip(edges, edges[1:])]
+
+
 class Hand:
     def __init__(self, place, send, sources, wholes, down, whole_down, scratch, sems):
         self.__dict__.update(place)
         self.send = send
         self.sources, self.wholes = sources, wholes
         self.down, self.whole_down = down, whole_down
-        self.passing, self.bounce, self.bounce_down = scratch
+        self.passing = scratch
         (
             self.s_plane,
             self.s_cross,
@@ -112,7 +124,7 @@
         ) = sems
         self.rows = sources[0].shape[0]
         self.width = wholes[0].shape[1]
-        self.part = self.rows // RELAY
+        self.part = far_part(self.rows)
         self.main = self.rows - self.part
         self.main_at = jnp.where(self.aligned, self.part, 0)
         self.over_at = jnp.where(self.aligned, self.main, 0)
@@ -137,11 +149,11 @@
         return self.sources[m].at[:, pl.ds(first, self.width)]
 
     def cross(self, m, side):
-        for k in range(RELAY - 1):
+        for k, (start, size) in enumerate(chunks(self.main)):
             self.send(
                 jnp.logical_not(self.aligned),
-                self.cols(m, k * self.part, self.part, side),
-                self.passing.at[m, side, k],
+                self.cols(m, start, size, side),
+                self.passing.at[m, side, pl.ds(start, size)],
                 self.s_cross.at[m, side, k],
                 self.r_cross.at[m, side, k],
                 self.here(self.peer),
@@ -192,43 +204,30 @@
                     self.here(to),
                 )
 
-    def fetches(self):
-        yield None, pltpu.make_async_copy(self.down, self.bounce_down, self.l_down)
+    def own_copies(self):
+        yield None, pltpu.make_async_copy(self.down, self.column(self.tp), self.l_down)
         for m in range(2):
             yield jnp.logical_and(self.aligned, self.primary), pltpu.make_async_copy(
-                self.own(m), self.bounce.at[m], self.l_own.at[m]
-            )
-
-    def puts(self):
-        yield None, pltpu.make_async_copy(
-            self.bounce_down, self.column(self.tp), self.l_down
-        )
-        for m in range(2):
-            yield jnp.logical_and(self.aligned, self.primary), pltpu.make_async_copy(
-                self.bounce.at[m], self.at(m, self.fs, 0, self.rows), self.l_own.at[m]
+                self.own(m), self.at(m, self.fs, 0, self.rows), self.l_own.at[m]
             )
 
     def keep(self):
-        for when, copy in self.fetches():
+        for when, copy in self.own_copies():
             guarded(when, copy.start)
-        for when, copy in self.fetches():
-            guarded(when, copy.wait)
-        for when, copy in self.puts():
-            guarded(when, copy.start)
 
     def kept(self):
-        for when, copy in self.puts():
+        for when, copy in self.own_copies():
             guarded(when, copy.wait)
 
     def relay(self, m, side):
         zone = (1 - self.x) * CORES + self.c
-        for k in range(RELAY - 1):
-            held = self.passing.at[m, side, k]
+        for k, (start, size) in enumerate(chunks(self.main)):
+            held = self.passing.at[m, side, pl.ds(start, size)]
             guarded(self.aligned, landed, held, self.r_cross.at[m, side, k])
             self.send(
                 self.aligned,
                 held,
-                self.at(m, self.fs, k * self.part, self.part),
+                self.at(m, self.fs, start, size),
                 self.s_pass.at[m, side, k],
                 self.r_main.at[m, self.fs],
                 (zone * SIDES + side, self.tp),
@@ -497,42 +496,16 @@
     return send, started
 
 
-def multiply(normed, plan, sums, partial_value, arrive, leave, others=()):
-    deep = plan[0][0].shape[0] // CUTS
-    wide = plan[2][0].shape[1] // CUTS
-
-    def cut(m, ref, k):
-        if m < 2:
-            return ref.at[pl.ds(k * deep, deep), :]
-        return ref.at[:, pl.ds(k * wide, wide)]
-
-    def coming(m, k):
-        src, held, _ = plan[m]
-        return pltpu.make_async_copy(cut(m, src, k), cut(m, held, k), arrive.at[m, k])
-
-    def going(m, k):
-        _, held, dst = plan[m]
-        return pltpu.make_async_copy(cut(m, held, k), cut(m, dst, k), leave.at[m, k])
-
-    def arrived(m, k):
-        coming(m, k).wait()
-        if plan[m][2] is not None:
-            going(m, k).start()
-
-    for k in range(CUTS):
-        coming(0, k).start()
-        coming(1, k).start()
-    for k in range(CUTS):
-        coming(2, k).start()
-    for copy in others:
-        copy.start()
+def multiply(normed, weights, sums, partial_value):
+    gate, up, down = weights
+    deep = gate.shape[0] // CUTS
+    wide = down.shape[1] // CUTS
     for k in range(CUTS):
         n = normed[:, k * deep : (k + 1) * deep]
-        for m, total in enumerate(sums):
-            arrived(m, k)
+        for weight, total in zip((gate, up), sums):
             term = jnp.dot(
                 n,
-                plan[m][1][k * deep : (k + 1) * deep, :],
+                weight[k * deep : (k + 1) * deep, :],
                 preferred_element_type=jnp.float32,
             )
             if k:
@@ -541,25 +514,21 @@
                 total[...] = term
     hidden = (jax.nn.silu(sums[0][...]) * sums[1][...]).astype(jnp.bfloat16)
     for k in range(CUTS):
-        arrived(2, k)
         partial_value[:, k * wide : (k + 1) * wide] = jnp.dot(
             hidden,
-            plan[2][1][:, k * wide : (k + 1) * wide],
+            down[:, k * wide : (k + 1) * wide],
             preferred_element_type=jnp.float32,
         ).astype(jnp.bfloat16)
-    return [
-        going(m, k) for m in range(3) if plan[m][2] is not None for k in range(CUTS)
-    ]
 
 
 def collect_kernel(*refs):
     (g1, u1, d1, g2, u2, d2, tokens, scales), refs = refs[:8], refs[8:]
     (w1, v1, x1, w2, v2, x2, out), refs = refs[:7], refs[7:]
-    (passing, bounce, bounce_down), refs = refs[:3], refs[3:]
-    (hold_gate, hold_up, hold_down, gate_sum, up_sum), refs = refs[:5], refs[5:]
+    passing, refs = refs[0], refs[1:]
+    (gate_sum, up_sum), refs = refs[:2], refs[2:]
     (normed, partial_value), refs = refs[:2], refs[2:]
     sems, refs = refs[:13], refs[13:]
-    arrive, close_scratches = refs[0], refs[1:]
+    close_scratches = refs
     place = placing()
     fs, tp = place["fs"], place["tp"]
     count = lax.axis_size("fs")
@@ -578,7 +547,7 @@
             (whole_gate, whole_up),
             down,
             whole_down,
-            (passing.at[h], bounce.at[h], bounce_down.at[h]),
+            passing.at[h],
             [sem.at[h] for sem in sems],
         )
         for h, (gate, up, down, whole_gate, whole_up, whole_down) in enumerate(
@@ -596,7 +565,6 @@
     one.home_block()
     two.cross(0, 0)
     two.plane_far(0, 0)
-    two.cross(0, 1)
     one.keep()
     one.relay(0, 0)
     one.whole_block(0, 0)
@@ -612,30 +580,30 @@
     one.whole_block(1, 3)
     for m, side in turns:
         two.plane_near(m, side)
-    two.send_down(aligned)
-    two.home_block()
     norm_rows(lambda some: tokens[some, :], normed)
     one.pass_down()
     for step in range(2 * SIDES):
         one.main_block(0, step)
+    two.home_block()
+    two.cross(0, 1)
     two.plane_far(0, 1)
     for step in range(2 * SIDES):
         one.main_block(1, step)
+    two.send_down(aligned)
     two.relay(0, 0)
-    for m in range(2):
-        for step in range(2 * SIDES):
-            one.minor_block(m, step)
+    for step in range(2 * SIDES):
+        one.minor_block(0, step)
+    for step in range(2 * SIDES):
+        one.minor_block(1, step)
+    two.relay(0, 1)
     one.second()
     one.kept()
-    two.relay(0, 1)
     two.cross(1, 0)
     multiply(
         normed,
-        ((w1, hold_gate, None), (v1, hold_up, None), (x1, hold_down, None)),
+        (w1, v1, x1),
         (gate_sum, up_sum),
         partial_value,
-        arrive,
-        None,
     )
     close.scatter()
     two.cross(1, 1)
@@ -655,15 +623,17 @@
     two.whole_block(1, 1)
     two.whole_block(1, 2)
     two.whole_block(1, 3)
+    two.pass_down()
+    for step in range(2 * SIDES):
+        two.main_block(0, step)
     close.side()
-    two.pass_down()
+    for step in range(2 * SIDES):
+        two.main_block(1, step)
     close.norm(normed, scales, out)
-    for m in range(2):
-        for step in range(2 * SIDES):
-            two.main_block(m, step)
-    for m in range(2):
-        for step in range(2 * SIDES):
-            two.minor_block(m, step)
+    for step in range(2 * SIDES):
+        two.minor_block(0, step)
+    for step in range(2 * SIDES):
+        two.minor_block(1, step)
     two.second()
     two.kept()
     for copy in started:
@@ -675,29 +645,24 @@
     rows, columns = gate.shape
     fs, tp = lax.axis_size("fs"), lax.axis_size("tp")
     width = columns * tp // fs
-    part = rows // RELAY
+    main = rows - far_part(rows)
     tall, wide = tokens.shape
-    whole = jax.ShapeDtypeStruct((rows * fs, width), jnp.bfloat16)
-    whole_down = jax.ShapeDtypeStruct((down.shape[0], down.shape[1] * tp), jnp.bfloat16)
+    whole = pltpu.VMEM((rows * fs, width), jnp.bfloat16)
+    whole_down = pltpu.VMEM((down.shape[0], down.shape[1] * tp), jnp.bfloat16)
     any_place = pl.BlockSpec(memory_space=pl.ANY)
     vmem = pl.BlockSpec(memory_space=pltpu.VMEM)
     dma = pltpu.SemaphoreType.DMA
     held = lambda *shape: pltpu.VMEM(shape, jnp.bfloat16)
-    relayed = dma((2, 2, SIDES, RELAY - 1))
+    relayed = dma((2, 2, SIDES, CHUNKS))
     by_owner = dma((2, 2, fs))
     *weights, normed_one = pl.pallas_call(
         collect_kernel,
         out_shape=(whole, whole, whole_down) * 2
         + (jax.ShapeDtypeStruct(tokens.shape, tokens.dtype),),
         in_specs=[any_place] * 6 + [vmem] * 2,
-        out_specs=(any_place,) * 6 + (vmem,),
+        out_specs=(vmem,) * 7,
         scratch_shapes=[
-            held(2, 2, SIDES, RELAY - 1, part, width),
-            held(2, 2, rows, width),
-            held(2, *down.shape),
-            held(*whole.shape),
-            held(*whole.shape),
-            held(*whole_down.shape),
+            held(2, 2, SIDES, main, width),
             pltpu.VMEM((tall, width), jnp.float32),
             pltpu.VMEM((tall, width), jnp.float32),
             held(tall, wide),
@@ -715,11 +680,10 @@
             dma((2, 3)),
             dma((2, 2)),
             dma((2,)),
-            dma((3, CUTS)),
             *close_scratch(tall, wide, fs),
         ],
         compiler_params=pltpu.CompilerParams(
-            has_side_effects=True, collective_id=0, vmem_limit_bytes=60 * 2**20
+            has_side_effects=True, collective_id=0, vmem_limit_bytes=COLLECT_VMEM
         ),
     )(*first, *second, tokens, scales[None, :])
     return weights[:3], weights[3:], normed_one
@@ -727,30 +691,15 @@
 
 def serve_kernel(*refs):
     normed, refs = refs[0], refs[1:]
-    first, second, refs = refs[:3], refs[3:6], refs[6:]
-    out_first, out_second, refs = refs[:3], refs[3:6], refs[6:]
-    partial_value, refs = refs[0], refs[1:]
-    held_first, held_second, refs = refs[:3], refs[3:6], refs[6:]
-    gate_sum, up_sum, arrive, leave, through, away = refs
-    ins = [
-        pltpu.make_async_copy(first[m], held_first[m], through.at[m]) for m in range(3)
+    weights, served, refs = refs[:6], refs[6:12], refs[12:]
+    partial_value, gate_sum, up_sum, leave = refs
+    copies = [
+        pltpu.make_async_copy(weights[m], served[m], leave.at[m]) for m in range(6)
     ]
-    outs = [
-        pltpu.make_async_copy(held_first[m], out_first[m], away.at[m]) for m in range(3)
-    ]
-    goings = multiply(
-        normed,
-        list(zip(second, held_second, out_second)),
-        (gate_sum, up_sum),
-        partial_value,
-        arrive,
-        leave,
-        ins,
-    )
-    for copy, next_copy in zip(ins, outs):
-        copy.wait()
-        next_copy.start()
-    for copy in goings + outs:
+    for copy in copies:
+        copy.start()
+    multiply(normed, weights[3:], (gate_sum, up_sum), partial_value)
+    for copy in copies:
         copy.wait()
 
 
@@ -760,27 +709,19 @@
     vmem = pl.BlockSpec(memory_space=pltpu.VMEM)
     any_place = pl.BlockSpec(memory_space=pl.ANY)
     same = lambda a: jax.ShapeDtypeStruct(a.shape, a.dtype)
-    dma = pltpu.SemaphoreType.DMA
     weights = (*first, *second)
+    sums = pltpu.VMEM((rows, gate.shape[1]), jnp.float32)
     *served, partial_value = pl.pallas_call(
         serve_kernel,
         out_shape=tuple(same(a) for a in weights) + (same(normed),),
-        in_specs=[vmem] + [any_place] * 6,
+        in_specs=[vmem] * 7,
         out_specs=(any_place,) * 6 + (vmem,),
-        scratch_shapes=[pltpu.VMEM(a.shape, a.dtype) for a in weights]
-        + [
-            pltpu.VMEM((rows, gate.shape[1]), jnp.float32),
-            pltpu.VMEM((rows, gate.shape[1]), jnp.float32),
-            dma((3, CUTS)),
-            dma((3, CUTS)),
-            dma((3,)),
-            dma((3,)),
-        ],
-        compiler_params=pltpu.CompilerParams(vmem_limit_bytes=60 * 2**20),
+        scratch_shapes=[sums, sums, pltpu.SemaphoreType.DMA((6,))],
+        compiler_params=pltpu.CompilerParams(vmem_limit_bytes=SERVE_VMEM),
         cost_estimate=pl.CostEstimate(
-            flops=6 * rows * gate.size, bytes_accessed=24 * gate.size, transcendentals=0
+            flops=6 * rows * gate.size, bytes_accessed=12 * gate.size, transcendentals=0
         ),
-    )(normed, *weights)
+    )(normed, *(pltpu.with_memory_space_constraint(a, pltpu.VMEM) for a in weights))
     return served[:3], served[3:], partial_value
 
 

time: 378 us -> 339 us (0.90)
  Pallas kernels: 359 us -> 316 us
    pallas_call x1, Pallas kernels: 293 us -> 255 us  [collect(): pl.pallas_call(collect_kernel, out_shape=(whole, whole, whole_down) * 2 +...]
    pallas_call x1, Pallas kernels: 25.9 us -> 12.4 us  [serve(): pl.pallas_call(serve_kernel, out_shape=tuple((same(a) for a in weights))...]
    pallas_call x1, Pallas kernels: 40.1 us -> 49.2 us  [close(): pl.pallas_call(close_kernel, out_shape=jax.ShapeDtypeStruct((rows, width)...]
where the time goes in v5:
time: 339 us; the launch traced here: 336 us
  Pallas kernels  316 us (93%)
  other arithmetic  12.6 us (4%)
  local copies, waits for them, and re-layouts  5.9 us (2%)
    pallas_call x1, Pallas kernels, collect(): pl.pallas_call(collect_kernel, out_shape=(whole, whole, whole_down) * 2 +...  255 us
    pallas_call x1, Pallas kernels, close(): pl.pallas_call(close_kernel, out_shape=jax.ShapeDtypeStruct((rows, width)...  49.2 us
    pallas_call x1, Pallas kernels, serve(): pl.pallas_call(serve_kernel, out_shape=tuple((same(a) for a in weights))...  12.4 us

profile of v5, /device:TPU:0, one launch (start us, length us, event | category | flops | bytes accessed | tf_op | source)
XLA Modules:
  0.0 335.6 jit_solution(14452366945196997344)
XLA Ops:
  0.6 0.8 dynamic_slice.8
  1.4 0.8 dynamic_slice.9
  2.2 0.0 copy-start.3
  2.2 0.0 copy-start.4
  2.2 3.3 convert_element_type.20.refs_2_
  5.5 0.0 copy-start.2
  5.5 3.3 convert_element_type.23.refs_5_
  8.9 0.0 copy-done.3
  8.9 0.0 copy-done.4
  8.9 0.0 copy-done.2
  8.9 5.9 %multiply_convert_fusion = (bf16[384,2048]{1,0:T(8,128)(2,1)}, bf16[384,2048]{1,0:T(8,128)(2,1)}, bf16[384,2048]{1,0:T(8,128)(2,1)}, bf16[384,2048]{1,0:T(8,128)(2,1)}) fusion(f32[384,2048]{1,0:T(8,128)S(1)} %copy-done.2, f32[384]{0:T(512)S(1)} %dynamic_slice.9, f32[384,2048]{1,0:T(8,128)S(1)} %copy-done.3, f32[384,2048]{1,0:T(8,128)S(1)} %copy-done.4, ...), kind=kLoop, calls=%fused_computation | loop fusion | flops 6291456 | bytes 18877440 | tf_op jit(solution)/shard_map/convert_element_type | solution.py:775
  14.8 254.8 %shard_map.144 = (bf16[3072,1024]{1,0:T(8,128)(2,1)S(1)}, bf16[3072,1024]{1,0:T(8,128)(2,1)S(1)}, bf16[1024,3072]{1,0:T(8,128)(2,1)S(1)}, bf16[3072,1024]{1,0:T(...) custom-call(bf16[384,2048]{1,0:T(8,128)(2,1)} %get-tuple-element.39.refs_, ...), custom_call_target="tpu_custom_call" | custom-call | tf_op jit(solution)/shard_map/pallas_call | solution.py:658
  269.6 0.0 copy-start
  269.6 1.2 copy-done
  270.8 12.4 %shard_map.145 = (bf16[3072,1024]{1,0:T(8,128)(2,1)}, bf16[3072,1024]{1,0:T(8,128)(2,1)}, bf16[1024,3072]{1,0:T(8,128)(2,1)}, bf16[3072,1024]{1,0:T(8,128)(2,1)}...) custom-call(bf16[160,3072]{1,0:T(8,128)(2,1)S(1)} %copy-done, ...), custom_call_target="tpu_custom_call" | custom-call | flops 3019898880 | bytes 37748736 | tf_op jit(solution)/shard_map/pallas_call | solution.py:714
  283.2 0.0 copy-start.1
  283.2 0.9 copy-done.1
  284.2 49.2 %shard_map.146 = bf16[160,3072]{1,0:T(8,128)(2,1)} custom-call(bf16[160,3072]{1,0:T(8,128)(2,1)} %copy-done.1, bf16[160,3072]{1,0:T(8,128)(2,1)} %get-tuple-element.21.refs_0_.normed, f32[1,3072]{1,0:T(1,128)} %bitcast.2), custom_call_target="tpu_custom_call" | custom-call | tf_op jit(solution)/shard_map/pallas_call | solution.py:748
  333.4 2.2 copy.17
Async XLA Ops:
  2.2 6.7 %copy-start.3 = (f32[384,2048]{1,0:T(8,128)S(1)}, f32[384,2048]{1,0:T(8,128)}, u32[]{:S(2)}) copy-start(f32[384,2048]{1,0:T(8,128)} %param.15) | copy-start | bytes 9437188
  2.2 6.7 %copy-start.4 = (f32[384,2048]{1,0:T(8,128)S(1)}, f32[384,2048]{1,0:T(8,128)}, u32[]{:S(2)}) copy-start(f32[384,2048]{1,0:T(8,128)} %param.12) | copy-start | bytes 9437188
  5.5 3.3 copy-start.2
  269.6 1.2 copy-start
  283.2 0.9 copy-start.1

commit v6 on v5

--- a/solution.py
+++ b/solution.py
@@ -10,7 +10,7 @@
 MESH = pl.DeviceIdType.MESH
 CORES = 2
 SIDES = 2
-COLLECT_VMEM = 20 * 2**20
+COLLECT_VMEM = 21 * 2**20
 SERVE_VMEM = 16 * 2**20
 CUTS = 4
 FAR = 5, 24
@@ -120,7 +120,6 @@
             self.s_down,
             self.r_down,
             self.l_own,
-            self.l_down,
         ) = sems
         self.rows = sources[0].shape[0]
         self.width = wholes[0].shape[1]
@@ -204,8 +203,38 @@
                     self.here(to),
                 )
 
+    def fold_down(self, trained, stage, sem):
+        lanes = self.down.shape[1]
+        mine = pl.ds(pl.multiple_of(self.tp * lanes, 128), lanes)
+
+        def put(rows, tile):
+            self.down[rows, :] = tile.astype(jnp.bfloat16)
+            self.whole_down[rows, mine] = tile.astype(jnp.bfloat16)
+
+        by_tiles(trained, stage, sem, put)
+
+    def fold_wide(self, m, trained, scales, stage, sem):
+        def put(rows, tile):
+            self.sources[m][rows, :] = (scales[rows, :] * tile).astype(jnp.bfloat16)
+
+        by_tiles(trained, stage, sem, put)
+
+    def keep_folded(self):
+        mine = pl.ds(pl.multiple_of(self.y * self.width, 128), self.width)
+
+        def tile(index, carry):
+            rows = pl.ds(pl.multiple_of(index * 16, 16), 16)
+            first = pl.multiple_of(self.fs * self.rows + index * 16, 16)
+            for m in range(2):
+                self.wholes[m][pl.ds(first, 16), :] = self.sources[m][rows, mine]
+            return carry
+
+        def block():
+            lax.fori_loop(0, self.rows // 16, tile, 0)
+
+        guarded(jnp.logical_and(self.aligned, self.primary), block)
+
     def own_copies(self):
-        yield None, pltpu.make_async_copy(self.down, self.column(self.tp), self.l_down)
         for m in range(2):
             yield jnp.logical_and(self.aligned, self.primary), pltpu.make_async_copy(
                 self.own(m), self.at(m, self.fs, 0, self.rows), self.l_own.at[m]
@@ -329,6 +358,10 @@
         pl.when(when)(functools.partial(act, *args))
 
 
+def beside_zone(zone):
+    return zone + 1 - 2 * (zone % 2)
+
+
 class Close:
     def __init__(self, place, send, partial_value, beside, halves, along, full, sems):
         self.__dict__.update(place)
@@ -346,6 +379,9 @@
             self.r_side,
         ) = sems
         self.zones = beside.shape[0]
+        self.near = beside_zone(self.z)
+        self.over = (self.z + 2) % self.zones
+        self.last = beside_zone(self.over)
 
     def piece(self, zone, side):
         width = self.full.shape[2]
@@ -396,6 +432,16 @@
             (self.z * SIDES + 1 - self.y, self.tp),
         )
 
+    def to_zone(self, kind, block, zone):
+        self.send(
+            None,
+            block,
+            block,
+            self.s_up.at[kind],
+            self.r_up.at[kind],
+            (zone * SIDES + self.y, self.tp),
+        )
+
     def spread(self):
         total = self.both_sides(0)
         for step in range(1, self.zones):
@@ -403,26 +449,25 @@
             total += self.along[step - 1].astype(jnp.float32)
         self.full[self.fs] = total.astype(jnp.bfloat16)
         block = self.held(self.z, self.y)
-        for step in range(1, self.zones):
-            self.send(
-                None,
-                block,
-                block,
-                self.s_up.at[step - 1],
-                self.r_up.at[step - 1],
-                (self.zone(step) * SIDES + self.y, self.tp),
-            )
+        self.to_zone(0, block, self.over)
+        self.to_zone(1, block, self.near)
         self.to_side(0, block)
 
+    def pass_on(self):
+        block = self.held(self.over, self.y)
+        landed(block, self.r_up.at[0])
+        self.to_zone(2, block, self.near)
+        self.to_side(1, block)
+
     def side(self):
-        for step in range(1, self.zones):
-            block = self.held(self.zone(-step), self.y)
-            landed(block, self.r_up.at[step - 1])
-            self.to_side(step, block)
+        for kind, zone in ((1, self.near), (2, self.last)):
+            block = self.held(zone, self.y)
+            landed(block, self.r_up.at[kind])
+            self.to_side(kind + 1, block)
 
     def norm(self, normed, scales, out):
-        for step in range(self.zones):
-            landed(self.held(self.zone(-step), 1 - self.y), self.r_side.at[step])
+        for step, zone in enumerate((self.z, self.over, self.near, self.last)):
+            landed(self.held(zone, 1 - self.y), self.r_side.at[step])
 
         def mixed(some):
             block = jnp.concatenate(
@@ -449,11 +494,37 @@
     lax.fori_loop(0, out.shape[0] // tall, some_rows, 0)
 
 
-def greet(partners):
+def greet(partners, meanwhile=None):
     barrier = pltpu.get_barrier_semaphore()
     for partner in partners:
         pl.semaphore_signal(barrier, inc=1, device_id=partner, device_id_type=MESH)
+    if meanwhile is not None:
+        meanwhile()
     pl.semaphore_wait(barrier, len(partners))
+
+
+def by_tiles(src, stage, sem, put):
+    tall = stage.shape[1]
+    count = src.shape[0] // tall
+
+    def fetch(k):
+        return pltpu.make_async_copy(
+            src.at[pl.ds(k * tall, tall), :], stage.at[k % 2], sem.at[k % 2]
+        )
+
+    fetch(0).start()
+    for k in range(count):
+        if k + 1 < count:
+            fetch(k + 1).start()
+        fetch(k).wait()
+
+        def tile(index, carry, k=k):
+            first = pl.multiple_of(index * 16, 16)
+            rows = pl.ds(pl.multiple_of(k * tall + index * 16, 16), 16)
+            put(rows, stage[k % 2, pl.ds(first, 16), :])
+            return carry
+
+        lax.fori_loop(0, tall // 16, tile, 0)
 
 
 def close_scratch(rows, width, count):
@@ -522,20 +593,17 @@
 
 
 def collect_kernel(*refs):
-    (g1, u1, d1, g2, u2, d2, tokens, scales), refs = refs[:8], refs[8:]
+    (g1, u1, t1, tg2, tu2, t2, tokens, scales, picked), refs = refs[:9], refs[9:]
     (w1, v1, x1, w2, v2, x2, out), refs = refs[:7], refs[7:]
-    passing, refs = refs[0], refs[1:]
+    (passing, folded, d1, d2), refs = refs[:4], refs[4:]
+    (stage_wide, stage_down, stage_sem), refs = refs[:3], refs[3:]
     (gate_sum, up_sum), refs = refs[:2], refs[2:]
     (normed, partial_value), refs = refs[:2], refs[2:]
-    sems, refs = refs[:13], refs[13:]
+    sems, refs = refs[:12], refs[12:]
     close_scratches = refs
     place = placing()
     fs, tp = place["fs"], place["tp"]
     count = lax.axis_size("fs")
-    greet(
-        [((fs + step) % count, tp) for step in range(1, count)]
-        + [(fs, place["peer"]), (fs, place["sibling"])]
-    )
     aligned = place["aligned"]
     unaligned = jnp.logical_not(aligned)
     send, started = sender()
@@ -551,11 +619,16 @@
             [sem.at[h] for sem in sems],
         )
         for h, (gate, up, down, whole_gate, whole_up, whole_down) in enumerate(
-            ((g1, u1, d1, w1, v1, x1), (g2, u2, d2, w2, v2, x2))
+            ((g1, u1, d1, w1, v1, x1), (folded.at[0], folded.at[1], d2, w2, v2, x2))
         )
     )
     close = Close(place, send, partial_value, *close_scratches[:4], close_scratches[4:])
     turns = [(m, side) for m in range(2) for side in range(SIDES)]
+    greet(
+        [((fs + step) % count, tp) for step in range(1, count)]
+        + [(fs, place["peer"]), (fs, place["sibling"])],
+        lambda: one.fold_down(t1, stage_down, stage_sem.at[0]),
+    )
 
     for m, side in turns:
         one.cross(m, side)
@@ -563,10 +636,14 @@
         one.plane_near(m, side)
     one.send_down(None)
     one.home_block()
+    one.keep()
+    one.relay(0, 0)
+    two.fold_wide(0, tg2, picked, stage_wide, stage_sem.at[1])
+    two.fold_wide(1, tu2, picked, stage_wide, stage_sem.at[1])
+    two.fold_down(t2, stage_down, stage_sem.at[0])
+    two.keep_folded()
     two.cross(0, 0)
     two.plane_far(0, 0)
-    one.keep()
-    one.relay(0, 0)
     one.whole_block(0, 0)
     one.whole_block(0, 1)
     one.relay(0, 1)
@@ -608,7 +685,6 @@
     close.scatter()
     two.cross(1, 1)
     two.send_down(unaligned)
-    two.keep()
     two.whole_block(0, 0)
     close.halve()
     two.plane_far(1, 0)
@@ -623,6 +699,7 @@
     two.whole_block(1, 1)
     two.whole_block(1, 2)
     two.whole_block(1, 3)
+    close.pass_on()
     two.pass_down()
     for step in range(2 * SIDES):
         two.main_block(0, step)
@@ -635,12 +712,11 @@
     for step in range(2 * SIDES):
         two.minor_block(1, step)
     two.second()
-    two.kept()
     for copy in started:
         copy.wait_send()
 
 
-def collect(first, second, tokens, scales):
+def collect(first, second, tokens, scales, picked):
     gate, _, down = first
     rows, columns = gate.shape
     fs, tp = lax.axis_size("fs"), lax.axis_size("tp")
@@ -658,11 +734,17 @@
     *weights, normed_one = pl.pallas_call(
         collect_kernel,
         out_shape=(whole, whole, whole_down) * 2
-        + (jax.ShapeDtypeStruct(tokens.shape, tokens.dtype),),
-        in_specs=[any_place] * 6 + [vmem] * 2,
+        + (pltpu.VMEM(tokens.shape, tokens.dtype),),
+        in_specs=[any_place] * 6 + [vmem] * 3,
         out_specs=(vmem,) * 7,
         scratch_shapes=[
             held(2, 2, SIDES, main, width),
+            held(2, *gate.shape),
+            held(*down.shape),
+            held(*down.shape),
+            pltpu.VMEM((2, gate.shape[0] // CUTS, gate.shape[1]), jnp.float32),
+            pltpu.VMEM((2, down.shape[0] // CUTS, down.shape[1]), jnp.float32),
+            dma((2, 2)),
             pltpu.VMEM((tall, width), jnp.float32),
             pltpu.VMEM((tall, width), jnp.float32),
             held(tall, wide),
@@ -679,14 +761,17 @@
             dma((2, 3)),
             dma((2, 3)),
             dma((2, 2)),
-            dma((2,)),
             *close_scratch(tall, wide, fs),
         ],
         compiler_params=pltpu.CompilerParams(
             has_side_effects=True, collective_id=0, vmem_limit_bytes=COLLECT_VMEM
         ),
-    )(*first, *second, tokens, scales[None, :])
+    )(*first, *second, tokens, scales[None, :], picked[:, None])
     return weights[:3], weights[3:], normed_one
+
+
+def in_vmem(*arrays):
+    return [pltpu.with_memory_space_constraint(a, pltpu.VMEM) for a in arrays]
 
 
 def serve_kernel(*refs):
@@ -713,7 +798,8 @@
     sums = pltpu.VMEM((rows, gate.shape[1]), jnp.float32)
     *served, partial_value = pl.pallas_call(
         serve_kernel,
-        out_shape=tuple(same(a) for a in weights) + (same(normed),),
+        out_shape=tuple(same(a) for a in weights)
+        + (pltpu.VMEM(normed.shape, normed.dtype),),
         in_specs=[vmem] * 7,
         out_specs=(any_place,) * 6 + (vmem,),
         scratch_shapes=[sums, sums, pltpu.SemaphoreType.DMA((6,))],
@@ -721,7 +807,7 @@
         cost_estimate=pl.CostEstimate(
             flops=6 * rows * gate.size, bytes_accessed=12 * gate.size, transcendentals=0
         ),
-    )(normed, *(pltpu.with_memory_space_constraint(a, pltpu.VMEM) for a in weights))
+    )(*in_vmem(normed, *weights))
     return served[:3], served[3:], partial_value
 
 
@@ -736,6 +822,7 @@
     close.scatter()
     close.halve()
     close.spread()
+    close.pass_on()
     close.side()
     close.norm(normed, scales, out)
     for copy in started:
@@ -747,12 +834,14 @@
     vmem = pl.BlockSpec(memory_space=pltpu.VMEM)
     return pl.pallas_call(
         close_kernel,
-        out_shape=jax.ShapeDtypeStruct((rows, width), jnp.bfloat16),
+        out_shape=pltpu.VMEM((rows, width), jnp.bfloat16),
         in_specs=[vmem] * 3,
         out_specs=vmem,
         scratch_shapes=close_scratch(rows, width, lax.axis_size("fs")),
-        compiler_params=pltpu.CompilerParams(has_side_effects=True, collective_id=1),
-    )(partial_value, normed, scales[None, :])
+        compiler_params=pltpu.CompilerParams(
+            has_side_effects=True, collective_id=1, vmem_limit_bytes=SERVE_VMEM
+        ),
+    )(*in_vmem(partial_value, normed), scales[None, :])
 
 
 def on_device(
@@ -769,27 +858,29 @@
 ):
     row_count = gate_first.shape[0]
     offset = lax.axis_index("fs") * row_count
+    pick = lambda scales: lax.dynamic_slice_in_dim(scales, offset, row_count, 0)
 
     def fold_gain(weight, scales):
-        picked = lax.dynamic_slice_in_dim(scales, offset, row_count, 0)
-        return (picked[:, None] * weight).astype(jnp.bfloat16)
-
-    first = (
-        fold_gain(gate_first, gain_first),
-        fold_gain(up_first, gain_first),
-        down_first.astype(jnp.bfloat16),
-    )
-    second = (
-        fold_gain(gate_second, gain_second),
-        fold_gain(up_second, gain_second),
-        down_second.astype(jnp.bfloat16),
-    )
+        return (pick(scales)[:, None] * weight).astype(jnp.bfloat16)
+
+    gate, up = fold_gain(gate_first, gain_first), fold_gain(up_first, gain_first)
     if use_kernels:
-        first, second, normed_one = collect(first, second, tokens, gain_first)
+        first, second, normed_one = collect(
+            (gate, up, down_first),
+            (gate_second, up_second, down_second),
+            tokens,
+            gain_first,
+            pick(gain_second),
+        )
         first, second, partial_value = serve(normed_one, first, second)
         result_rows = close(partial_value, normed_one, gain_second)
     else:
-        first, second = collect_plain(*first), collect_plain(*second)
+        first = collect_plain(gate, up, down_first.astype(jnp.bfloat16))
+        second = collect_plain(
+            fold_gain(gate_second, gain_second),
+            fold_gain(up_second, gain_second),
+            down_second.astype(jnp.bfloat16),
+        )
         normed_zero = plain_norm(tokens).astype(jnp.bfloat16)
         normed_one = half_step_plain(normed_zero, gain_first, *first)
         result_rows = half_step_plain(normed_one, gain_second, *second)

time: 339 us -> 322 us (0.950)
  other arithmetic: 12.6 us -> 5.48 us
  Pallas kernels: 316 us -> 310 us
    pallas_call x1, Pallas kernels: 49.2 us -> 41.3 us  [close(): pl.pallas_call(close_kernel, out_shape=pltpu.VMEM((rows, width), jnp.bflo...]
    convert_element_type x3 -> x1, other arithmetic: 12.6 us -> 5.48 us  [fold_gain(): return (pick(scales)[:, None] * weight).astype(jnp.bfloat16)]
    unnamed x11 -> x3, local copies, waits for them, and re-layouts: 4.35 us -> 0.95 us
where the time goes in v6:
time: 322 us; the launch traced here: 320 us
  Pallas kernels  310 us (96%)
  other arithmetic  5.48 us (2%)
  local copies, waits for them, and re-layouts  3.3 us (1%)
    pallas_call x1, Pallas kernels, collect(): pl.pallas_call(collect_kernel, out_shape=(whole, whole, whole_down) * 2 +...  256 us
    pallas_call x1, Pallas kernels, close(): pl.pallas_call(close_kernel, out_shape=pltpu.VMEM((rows, width), jnp.bflo...  41.3 us
    pallas_call x1, Pallas kernels, serve(): pl.pallas_call(serve_kernel, out_shape=tuple((same(a) for a in weights))...  12.4 us

profile of v6, /device:TPU:0, one launch (start us, length us, event | category | flops | bytes accessed | tf_op | source)
XLA Modules:
  0.0 319.7 jit_solution(2157111238901362918)
XLA Ops:
  0.6 0.8 dynamic_slice.7
  1.4 0.8 dynamic_slice.8
  2.2 0.8 broadcast_in_dim.14.refs_8_
  3.0 5.5 %multiply_convert_fusion = (bf16[384,2048]{1,0:T(8,128)(2,1)}, bf16[384,2048]{1,0:T(8,128)(2,1)}) fusion(f32[384,2048]{1,0:T(8,128)} %param.13, f32[384]{0:T(512)S(1)} %dynamic_slice.7, f32[384,2048]{1,0:T(8,128)} %param.12), kind=kLoop, calls=%fused_computation | loop fusion | flops 3145728 | bytes 9438720 | tf_op jit(solution)/shard_map/convert_element_type | solution.py:864
  8.5 256.5 %shard_map.144 = (bf16[3072,1024]{1,0:T(8,128)(2,1)S(1)}, bf16[3072,1024]{1,0:T(8,128)(2,1)S(1)}, bf16[1024,3072]{1,0:T(8,128)(2,1)S(1)}, bf16[3072,1024]{1,0:T(...) custom-call(bf16[384,2048]{1,0:T(8,128)(2,1)} %get-tuple-element.36.r, ...), custom_call_target="tpu_custom_call" | custom-call | tf_op jit(solution)/shard_map/pallas_call | solution.py:734
  264.9 0.0 copy-start
  265.0 12.4 %shard_map.145 = (bf16[3072,1024]{1,0:T(8,128)(2,1)}, bf16[3072,1024]{1,0:T(8,128)(2,1)}, bf16[1024,3072]{1,0:T(8,128)(2,1)}, bf16[3072,1024]{1,0:T(8,128)(2,1)}...) custom-call(bf16[160,3072]{1,0:T(8,128)(2,1)S(1)} %get-tuple-element.21.refs_0_.normed, ...), custom_call_target="tpu_custom_call" | custom-call | flops 3019898880 | bytes 37748736 | tf_op jit(solution)/shard_map/pallas_call | solution.py:799
  277.4 0.0 copy-done
  277.4 41.3 %shard_map.146 = bf16[160,3072]{1,0:T(8,128)(2,1)S(1)} custom-call(bf16[160,3072]{1,0:T(8,128)(2,1)S(1)} %get-tuple-element.28.partial_value, bf16[160,3072]{1,0:T(8,128)(2,1)S(1)} %get-tuple-element.21.refs_0_.normed, f32[1,3072]{1,0:T(1,128)S(1)} %bitcast.2), custom_call_target="tpu_custom_call" | custom-call | tf_op jit(solution)/shard_map/pallas_call | solution.py:835
  318.7 0.9 copy.18
Async XLA Ops:
  264.9 12.4 %copy-start = (f32[3072]{0:T(1024)S(1)}, f32[3072]{0:T(1024)}, u32[]{:S(2)}) copy-start(f32[3072]{0:T(1024)} %param.11) | copy-start | bytes 36868

commit v7 on v6

--- a/solution.py
+++ b/solution.py
@@ -10,8 +10,8 @@
 MESH = pl.DeviceIdType.MESH
 CORES = 2
 SIDES = 2
-COLLECT_VMEM = 21 * 2**20
-SERVE_VMEM = 16 * 2**20
+COLLECT_VMEM = 24 * 2**20
+SERVE_VMEM = 24 * 2**20
 CUTS = 4
 FAR = 5, 24
 CHUNKS = 4
@@ -119,7 +119,6 @@
             self.s_over,
             self.s_down,
             self.r_down,
-            self.l_own,
         ) = sems
         self.rows = sources[0].shape[0]
         self.width = wholes[0].shape[1]
@@ -233,20 +232,6 @@
             lax.fori_loop(0, self.rows // 16, tile, 0)
 
         guarded(jnp.logical_and(self.aligned, self.primary), block)
-
-    def own_copies(self):
-        for m in range(2):
-            yield jnp.logical_and(self.aligned, self.primary), pltpu.make_async_copy(
-                self.own(m), self.at(m, self.fs, 0, self.rows), self.l_own.at[m]
-            )
-
-    def keep(self):
-        for when, copy in self.own_copies():
-            guarded(when, copy.start)
-
-    def kept(self):
-        for when, copy in self.own_copies():
-            guarded(when, copy.wait)
 
     def relay(self, m, side):
         zone = (1 - self.x) * CORES + self.c
@@ -593,13 +578,13 @@
 
 
 def collect_kernel(*refs):
-    (g1, u1, t1, tg2, tu2, t2, tokens, scales, picked), refs = refs[:9], refs[9:]
+    (tg1, tu1, t1, tg2, tu2, t2, tokens, scales, picks), refs = refs[:9], refs[9:]
     (w1, v1, x1, w2, v2, x2, out), refs = refs[:7], refs[7:]
     (passing, folded, d1, d2), refs = refs[:4], refs[4:]
     (stage_wide, stage_down, stage_sem), refs = refs[:3], refs[3:]
     (gate_sum, up_sum), refs = refs[:2], refs[2:]
     (normed, partial_value), refs = refs[:2], refs[2:]
-    sems, refs = refs[:12], refs[12:]
+    sems, refs = refs[:11], refs[11:]
     close_scratches = refs
     place = placing()
     fs, tp = place["fs"], place["tp"]
@@ -619,27 +604,38 @@
             [sem.at[h] for sem in sems],
         )
         for h, (gate, up, down, whole_gate, whole_up, whole_down) in enumerate(
-            ((g1, u1, d1, w1, v1, x1), (folded.at[0], folded.at[1], d2, w2, v2, x2))
+            (
+                (folded.at[0], folded.at[1], d1, w1, v1, x1),
+                (folded.at[2], folded.at[3], d2, w2, v2, x2),
+            )
         )
     )
     close = Close(place, send, partial_value, *close_scratches[:4], close_scratches[4:])
     turns = [(m, side) for m in range(2) for side in range(SIDES)]
+
+    def first_folds():
+        one.fold_wide(0, tg1, picks.at[0], stage_wide, stage_sem.at[1])
+
     greet(
         [((fs + step) % count, tp) for step in range(1, count)]
         + [(fs, place["peer"]), (fs, place["sibling"])],
-        lambda: one.fold_down(t1, stage_down, stage_sem.at[0]),
+        first_folds,
     )
 
-    for m, side in turns:
-        one.cross(m, side)
-        one.plane_far(m, side)
-        one.plane_near(m, side)
+    for m in range(2):
+        if m:
+            one.fold_wide(1, tu1, picks.at[0], stage_wide, stage_sem.at[1])
+        for side in range(SIDES):
+            one.cross(m, side)
+            one.plane_far(m, side)
+            one.plane_near(m, side)
+    one.fold_down(t1, stage_down, stage_sem.at[0])
     one.send_down(None)
     one.home_block()
-    one.keep()
+    one.keep_folded()
     one.relay(0, 0)
-    two.fold_wide(0, tg2, picked, stage_wide, stage_sem.at[1])
-    two.fold_wide(1, tu2, picked, stage_wide, stage_sem.at[1])
+    two.fold_wide(0, tg2, picks.at[1], stage_wide, stage_sem.at[1])
+    two.fold_wide(1, tu2, picks.at[1], stage_wide, stage_sem.at[1])
     two.fold_down(t2, stage_down, stage_sem.at[0])
     two.keep_folded()
     two.cross(0, 0)
@@ -664,17 +660,16 @@
     two.home_block()
     two.cross(0, 1)
     two.plane_far(0, 1)
+    two.relay(0, 0)
     for step in range(2 * SIDES):
         one.main_block(1, step)
     two.send_down(aligned)
-    two.relay(0, 0)
     for step in range(2 * SIDES):
         one.minor_block(0, step)
     for step in range(2 * SIDES):
         one.minor_block(1, step)
     two.relay(0, 1)
     one.second()
-    one.kept()
     two.cross(1, 0)
     multiply(
         normed,
@@ -716,7 +711,7 @@
         copy.wait_send()
 
 
-def collect(first, second, tokens, scales, picked):
+def collect(first, second, tokens, scales, picks):
     gate, _, down = first
     rows, columns = gate.shape
     fs, tp = lax.axis_size("fs"), lax.axis_size("tp")
@@ -739,7 +734,7 @@
         out_specs=(vmem,) * 7,
         scratch_shapes=[
             held(2, 2, SIDES, main, width),
-            held(2, *gate.shape),
+            held(4, *gate.shape),
             held(*down.shape),
             held(*down.shape),
             pltpu.VMEM((2, gate.shape[0] // CUTS, gate.shape[1]), jnp.float32),
@@ -760,13 +755,12 @@
             by_owner,
             dma((2, 3)),
             dma((2, 3)),
-            dma((2, 2)),
             *close_scratch(tall, wide, fs),
         ],
         compiler_params=pltpu.CompilerParams(
             has_side_effects=True, collective_id=0, vmem_limit_bytes=COLLECT_VMEM
         ),
-    )(*first, *second, tokens, scales[None, :], picked[:, None])
+    )(*first, *second, tokens, scales[None, :], picks[:, :, None])
     return weights[:3], weights[3:], normed_one
 
 
@@ -863,19 +857,22 @@
     def fold_gain(weight, scales):
         return (pick(scales)[:, None] * weight).astype(jnp.bfloat16)
 
-    gate, up = fold_gain(gate_first, gain_first), fold_gain(up_first, gain_first)
     if use_kernels:
         first, second, normed_one = collect(
-            (gate, up, down_first),
+            (gate_first, up_first, down_first),
             (gate_second, up_second, down_second),
             tokens,
             gain_first,
-            pick(gain_second),
+            jnp.stack([pick(gain_first), pick(gain_second)]),
         )
         first, second, partial_value = serve(normed_one, first, second)
         result_rows = close(partial_value, normed_one, gain_second)
     else:
-        first = collect_plain(gate, up, down_first.astype(jnp.bfloat16))
+        first = collect_plain(
+            fold_gain(gate_first, gain_first),
+            fold_gain(up_first, gain_first),
+            down_first.astype(jnp.bfloat16),
+        )
         second = collect_plain(
             fold_gain(gate_second, gain_second),
             fold_gain(up_second, gain_second),

time: 322 us -> 313 us (0.972)
  other arithmetic: 5.48 us -> 0.01 us
  Pallas kernels: 310 us -> 306 us
    convert_element_type x1 -> x0, other arithmetic: 5.48 us -> none  [fold_gain(): return (pick(scales)[:, None] * weight).astype(jnp.bfloat16)]
    pallas_call x1, Pallas kernels: 41.3 us -> 35.9 us  [close(): pl.pallas_call(close_kernel, out_shape=pltpu.VMEM((rows, width), jnp.bflo...]
where the time goes in v7:
time: 313 us; the launch traced here: 310 us
  Pallas kernels  306 us (98%)
  local copies, waits for them, and re-layouts  3.45 us (1%)
    pallas_call x1, Pallas kernels, collect(): pl.pallas_call(collect_kernel, out_shape=(whole, whole, whole_down) * 2 +...  258 us
    pallas_call x1, Pallas kernels, close(): pl.pallas_call(close_kernel, out_shape=pltpu.VMEM((rows, width), jnp.bflo...  35.9 us
    pallas_call x1, Pallas kernels, serve(): pl.pallas_call(serve_kernel, out_shape=tuple((same(a) for a in weights))...  12.4 us

profile of v7, /device:TPU:0, one launch (start us, length us, event | category | flops | bytes accessed | tf_op | source)
XLA Modules:
  0.0 310.2 jit_solution(11186248575467508318)
XLA Ops:
  0.6 0.8 dynamic_slice.6
  1.4 0.8 dynamic_slice.7
  2.2 0.9 copy.16.refs_8_
  3.2 257.8 %shard_map.144 = (bf16[3072,1024]{1,0:T(8,128)(2,1)S(1)}, bf16[3072,1024]{1,0:T(8,128)(2,1)S(1)}, bf16[1024,3072]{1,0:T(8,128)(2,1)S(1)}, bf16[3072,1024]{1,0:T(...) custom-call(f32[384,2048]{1,0:T(8,128)} %refs_0_.1, ...), custom_call_target="tpu_custom_call" | custom-call | tf_op jit(solution)/shard_map/pallas_call | solution.py:729
  260.9 0.0 copy-start
  260.9 12.4 %shard_map.145 = (bf16[3072,1024]{1,0:T(8,128)(2,1)}, bf16[3072,1024]{1,0:T(8,128)(2,1)}, bf16[1024,3072]{1,0:T(8,128)(2,1)}, bf16[3072,1024]{1,0:T(8,128)(2,1)}...) custom-call(bf16[160,3072]{1,0:T(8,128)(2,1)S(1)} %get-tuple-element.21.refs_0_.normed, ...), custom_call_target="tpu_custom_call" | custom-call | flops 3019898880 | bytes 37748736 | tf_op jit(solution)/shard_map/pallas_call | solution.py:793
  273.3 0.0 copy-done
  273.3 35.9 %shard_map.146 = bf16[160,3072]{1,0:T(8,128)(2,1)S(1)} custom-call(bf16[160,3072]{1,0:T(8,128)(2,1)S(1)} %get-tuple-element.28.partial_value, bf16[160,3072]{1,0:T(8,128)(2,1)S(1)} %get-tuple-element.21.refs_0_.normed, f32[1,3072]{1,0:T(1,128)S(1)} %bitcast.4), custom_call_target="tpu_custom_call" | custom-call | tf_op jit(solution)/shard_map/pallas_call | solution.py:829
  309.3 0.9 copy.18
  (3 shorter events, 0.0 us)
Async XLA Ops:
  260.9 12.4 %copy-start = (f32[3072]{0:T(1024)S(1)}, f32[3072]{0:T(1024)}, u32[]{:S(2)}) copy-start(f32[3072]{0:T(1024)} %param.11) | copy-start | bytes 36868

commit v8 on v7

--- a/solution.py
+++ b/solution.py
@@ -578,7 +578,8 @@
 
 
 def collect_kernel(*refs):
-    (tg1, tu1, t1, tg2, tu2, t2, tokens, scales, picks), refs = refs[:9], refs[9:]
+    (tg1, tu1, t1, tg2, tu2, t2, tokens, scales), refs = refs[:8], refs[8:]
+    picks, refs = refs[:2], refs[2:]
     (w1, v1, x1, w2, v2, x2, out), refs = refs[:7], refs[7:]
     (passing, folded, d1, d2), refs = refs[:4], refs[4:]
     (stage_wide, stage_down, stage_sem), refs = refs[:3], refs[3:]
@@ -614,7 +615,7 @@
     turns = [(m, side) for m in range(2) for side in range(SIDES)]
 
     def first_folds():
-        one.fold_wide(0, tg1, picks.at[0], stage_wide, stage_sem.at[1])
+        one.fold_wide(0, tg1, picks[0], stage_wide, stage_sem.at[1])
 
     greet(
         [((fs + step) % count, tp) for step in range(1, count)]
@@ -624,7 +625,7 @@
 
     for m in range(2):
         if m:
-            one.fold_wide(1, tu1, picks.at[0], stage_wide, stage_sem.at[1])
+            one.fold_wide(1, tu1, picks[0], stage_wide, stage_sem.at[1])
         for side in range(SIDES):
             one.cross(m, side)
             one.plane_far(m, side)
@@ -634,8 +635,8 @@
     one.home_block()
     one.keep_folded()
     one.relay(0, 0)
-    two.fold_wide(0, tg2, picks.at[1], stage_wide, stage_sem.at[1])
-    two.fold_wide(1, tu2, picks.at[1], stage_wide, stage_sem.at[1])
+    two.fold_wide(0, tg2, picks[1], stage_wide, stage_sem.at[1])
+    two.fold_wide(1, tu2, picks[1], stage_wide, stage_sem.at[1])
     two.fold_down(t2, stage_down, stage_sem.at[0])
     two.keep_folded()
     two.cross(0, 0)
@@ -730,7 +731,7 @@
         collect_kernel,
         out_shape=(whole, whole, whole_down) * 2
         + (pltpu.VMEM(tokens.shape, tokens.dtype),),
-        in_specs=[any_place] * 6 + [vmem] * 3,
+        in_specs=[any_place] * 6 + [vmem] * 4,
         out_specs=(vmem,) * 7,
         scratch_shapes=[
             held(2, 2, SIDES, main, width),
@@ -760,7 +761,7 @@
         compiler_params=pltpu.CompilerParams(
             has_side_effects=True, collective_id=0, vmem_limit_bytes=COLLECT_VMEM
         ),
-    )(*first, *second, tokens, scales[None, :], picks[:, :, None])
+    )(*first, *second, tokens, scales[None, :], *(pick[:, None] for pick in picks))
     return weights[:3], weights[3:], normed_one
 
 
@@ -863,7 +864,7 @@
             (gate_second, up_second, down_second),
             tokens,
             gain_first,
-            jnp.stack([pick(gain_first), pick(gain_second)]),
+            (pick(gain_first), pick(gain_second)),
         )
         first, second, partial_value = serve(normed_one, first, second)
         result_rows = close(partial_value, normed_one, gain_second)

time: 313 us -> 314 us (level)
  no operation moved by 1% of the time
where the time goes in v8:
time: 314 us; the launch traced here: 311 us
  Pallas kernels  306 us (97%)
  local copies, waits for them, and re-layouts  4.09 us (1%)
    pallas_call x1, Pallas kernels, collect(): pl.pallas_call(collect_kernel, out_shape=(whole, whole, whole_down) * 2 +...  258 us
    pallas_call x1, Pallas kernels, close(): pl.pallas_call(close_kernel, out_shape=pltpu.VMEM((rows, width), jnp.bflo...  35.9 us
    pallas_call x1, Pallas kernels, serve(): pl.pallas_call(serve_kernel, out_shape=tuple((same(a) for a in weights))...  12.4 us

profile of v8, /device:TPU:0, one launch (start us, length us, event | category | flops | bytes accessed | tf_op | source)
XLA Modules:
  0.0 310.8 jit_solution(3922360298180105911)
XLA Ops:
  0.6 0.8 dynamic_slice.6
  1.4 0.8 dynamic_slice.7
  2.2 0.8 broadcast_in_dim.17.refs_9_
  3.0 0.8 broadcast_in_dim.16.refs_8_
  3.8 257.8 %shard_map.144 = (bf16[3072,1024]{1,0:T(8,128)(2,1)S(1)}, bf16[3072,1024]{1,0:T(8,128)(2,1)S(1)}, bf16[1024,3072]{1,0:T(8,128)(2,1)S(1)}, bf16[3072,1024]{1,0:T(...) custom-call(f32[384,2048]{1,0:T(8,128)} %refs_0_.1, ...), custom_call_target="tpu_custom_call" | custom-call | tf_op jit(solution)/shard_map/pallas_call | solution.py:730
  261.5 0.0 copy-start
  261.5 12.4 %shard_map.145 = (bf16[3072,1024]{1,0:T(8,128)(2,1)}, bf16[3072,1024]{1,0:T(8,128)(2,1)}, bf16[1024,3072]{1,0:T(8,128)(2,1)}, bf16[3072,1024]{1,0:T(8,128)(2,1)}...) custom-call(bf16[160,3072]{1,0:T(8,128)(2,1)S(1)} %get-tuple-element.21.refs_0_.normed, ...), custom_call_target="tpu_custom_call" | custom-call | flops 3019898880 | bytes 37748736 | tf_op jit(solution)/shard_map/pallas_call | solution.py:794
  274.0 0.0 copy-done
  274.0 35.9 %shard_map.146 = bf16[160,3072]{1,0:T(8,128)(2,1)S(1)} custom-call(bf16[160,3072]{1,0:T(8,128)(2,1)S(1)} %get-tuple-element.28.partial_value, bf16[160,3072]{1,0:T(8,128)(2,1)S(1)} %get-tuple-element.21.refs_0_.normed, f32[1,3072]{1,0:T(1,128)S(1)} %bitcast.2), custom_call_target="tpu_custom_call" | custom-call | tf_op jit(solution)/shard_map/pallas_call | solution.py:830
  309.9 0.9 copy.19
Async XLA Ops:
  261.5 12.4 %copy-start = (f32[3072]{0:T(1024)S(1)}, f32[3072]{0:T(1024)}, u32[]{:S(2)}) copy-start(f32[3072]{0:T(1024)} %param.11) | copy-start | bytes 36868
